TPU v7x, 32 devices: a whole 2x2x4 slice. The times are simulated.
32 devices in a mesh: ep: 8 (over z, x), tp: 4 (over y, core).
Axes of the slice: x: 2, y: 2, z: 4, core: 2. Of those that a mesh axis runs over, the one named last changes fastest.
Arguments:
- tokens: bfloat16 [2048, 2048], P('ep'), may hold values from -6 to 6
- routes: int32 [2048, 4], P('ep'), may hold values from 0 to 7, all different within a row; in each aligned block of 256 rows (0 to 255, 256 to 511, ...) at most 160 rows name the same one
- gate_weights: float32 [2048, 4], P('ep'), may hold values from 0.05 to 1
- out_grad: bfloat16 [2048, 2048], P('ep'), may hold values from -0.59765625 to 0.59765625
- w_gate: bfloat16 [8, 2048, 1024], P('ep', None, 'tp'), may hold values from -0.1875 to 0.1875
- w_up: bfloat16 [8, 2048, 1024], P('ep', None, 'tp'), may hold values from -0.1875 to 0.1875
- w_down: bfloat16 [8, 1024, 2048], P('ep', 'tp'), may hold values from -0.1875 to 0.1875
Outputs:
- token_grad: bfloat16 [2048, 2048], P('ep', 'tp')
- gate_grad: float32 [2048, 4], P('ep')
- gate_weight_grad: float32 [8, 2048, 1024], P('ep', None, 'tp')
- up_weight_grad: float32 [8, 2048, 1024], P('ep', None, 'tp')
- down_weight_grad: float32 [8, 1024, 2048], P('ep', 'tp')
Inputs may be any that keep to these rules, and one draw needn't show every extreme that they name: `routes`: each row names 4 different experts. In each aligned block of 256 rows (the rows of one device) no expert is named by more than 160 rows, and in some block an expert is named by exactly 160 rows.
All inputs are finite; a program needn't handle non-finite values.
Results may differ from a plain program's by a relative error of at most 0.012.
Values may be sent and summed in bfloat16 or wider, within the bound.
A program may use at most 128 MiB of HBM per device.

v0:
```python
import jax
import jax.numpy as jnp
from jax import lax
from jax.experimental import pallas as pl
from jax.experimental.pallas import tpu as pltpu
from jax.sharding import PartitionSpec as P

clamp_limit = 7.0
sigmoid_slope = 1.702
MESH = pl.DeviceIdType.MESH


def partners():
    ep_count = lax.axis_size("ep")
    tp_count = lax.axis_size("tp")
    here = lax.axis_index("ep")
    part = lax.axis_index("tp")
    beside = part + 1 - 2 * (part % 2)
    across = (part + tp_count // 2) % tp_count
    return ep_count, here, part, beside, across


def greet(ep_count, here, part, beside, across):
    barrier = pltpu.get_barrier_semaphore()
    pl.semaphore_signal(barrier, inc=1, device_id=(here, beside), device_id_type=MESH)
    pl.semaphore_signal(barrier, inc=1, device_id=(here, across), device_id_type=MESH)

    def call(j, carry):
        peer = (here + j) % ep_count
        pl.semaphore_signal(barrier, inc=1, device_id=(peer, part), device_id_type=MESH)
        return carry

    lax.fori_loop(1, ep_count, call, 0)
    pl.semaphore_wait(barrier, ep_count + 1)


def remote(src, dst, sent, got, device):
    return pltpu.make_async_remote_copy(
        src_ref=src, dst_ref=dst, send_sem=sent, recv_sem=got, device_id=device, device_id_type=MESH
    )


def dispatch_kernel(
    token_ref, grad_ref, weight_ref, token_rows, grad_rows, weights_out,
    s1, r1, s2, r2, s3, r3, s4, r4, sw, rw, own_sem,
):
    ep_count, here, part, beside, across = partners()
    width = token_ref.shape[2]
    pairs = ((0, token_ref, token_rows), (1, grad_ref, grad_rows))

    def block(rows_ref, source, owner):
        columns = pl.ds(pl.multiple_of(owner * width, width), width)
        return rows_ref.at[source, :, columns]

    greet(ep_count, here, part, beside, across)

    def first(j):
        peer = (here + j) % ep_count
        return [
            remote(send.at[peer], block(rows, here, part), s1.at[i, j], r1.at[i, j], (peer, part))
            for i, send, rows in pairs
        ]

    def first_weight(j):
        peer = (here + j) % ep_count
        return remote(
            weight_ref.at[peer], weights_out.at[here], sw.at[j], rw.at[j], (peer, part)
        )

    def forward(j, owner, sent, got, to):
        source = (here + ep_count - j) % ep_count
        return [
            remote(
                block(rows, source, owner), block(rows, source, owner),
                sent.at[i, j], got.at[i, j], (here, to),
            )
            for i, _, rows in pairs
        ]

    def near(j):
        return forward(j, part, s2, r2, beside)

    def far(j):
        return forward(j, part, s3, r3, across)

    def onward(j):
        return forward(j, across, s4, r4, beside)

    owns = [
        pltpu.make_async_copy(send.at[here], block(rows, here, part), own_sem.at[i])
        for i, send, rows in pairs
    ]
    owns.append(pltpu.make_async_copy(weight_ref.at[here], weights_out.at[here], own_sem.at[2]))
    for copy in owns:
        copy.start()

    def launch(j, carry):
        first_weight(j).start()
        for copy in first(j):
            copy.start()
        return carry

    lax.fori_loop(1, ep_count, launch, 0)
    for copy in owns:
        copy.wait()
    for copy in far(0) + near(0):
        copy.start()

    def pass_on(j, carry):
        @pl.when(j < ep_count)
        def _():
            for i in range(2):
                first(j)[i].wait_recv()
                far(j)[i].start()
                near(j)[i].start()

        @pl.when(j >= 2)
        def _():
            for i in range(2):
                far(j - 2)[i].wait_recv()
                onward(j - 2)[i].start()

        return carry

    lax.fori_loop(1, ep_count + 2, pass_on, 0)

    def finish(j, carry):
        for i in range(2):
            near(j)[i].wait()
            onward(j)[i].wait()
            far(j)[i].wait_send()

        @pl.when(j >= 1)
        def _():
            for copy in first(j):
                copy.wait_send()
            first_weight(j).wait()

        return carry

    lax.fori_loop(0, ep_count, finish, 0)


def dispatch(send_tokens, send_grads, weights, model_width):
    ep_count, capacity, width = send_tokens.shape
    sems = [pltpu.SemaphoreType.DMA((2, ep_count)) for _ in range(8)]
    sems += [pltpu.SemaphoreType.DMA((ep_count,)) for _ in range(2)]
    whole = jax.ShapeDtypeStruct((ep_count, capacity, model_width), jnp.bfloat16)
    return pl.pallas_call(
        dispatch_kernel,
        out_shape=(whole, whole, jax.ShapeDtypeStruct(weights.shape, jnp.float32)),
        in_specs=[pl.BlockSpec(memory_space=pltpu.VMEM)] * 3,
        out_specs=(
            pl.BlockSpec(memory_space=pl.ANY),
            pl.BlockSpec(memory_space=pl.ANY),
            pl.BlockSpec(memory_space=pltpu.VMEM),
        ),
        scratch_shapes=sems + [pltpu.SemaphoreType.DMA((3,))],
        compiler_params=pltpu.CompilerParams(collective_id=0, has_side_effects=True),
    )(send_tokens, send_grads, weights)


def combine_kernel(
    rows_ref, product_ref, back_ref, back_product, near_buf, far_send, far_buf, last_send,
    product_near, product_sum, product_far, product_send,
    s1, r1, s2, r2, s3, r3, sw, rw, small_send, small_recv,
):
    ep_count, here, part, beside, across = partners()
    width = back_ref.shape[2]
    beside_far = (beside + lax.axis_size("tp") // 2) % lax.axis_size("tp")

    def columns(owner):
        return pl.ds(pl.multiple_of(owner * width, width), width)

    greet(ep_count, here, part, beside, across)

    def near(which, j):
        target = (here + j) % ep_count
        owner = beside_far if which == 0 else beside
        return remote(
            rows_ref.at[target, :, columns(owner)], near_buf.at[which, j],
            s1.at[which, j], r1.at[which, j], (here, beside),
        )

    def far(j):
        return remote(far_send.at[j], far_buf.at[j], s2.at[j], r2.at[j], (here, across))

    def last(j):
        peer = (here + j) % ep_count
        return remote(last_send.at[j], back_ref.at[here], s3.at[j], r3.at[j], (peer, part))

    def last_product(j):
        peer = (here + j) % ep_count
        return remote(
            product_send.at[peer], back_product.at[here], sw.at[j], rw.at[j], (peer, part)
        )

    small_near = remote(product_ref, product_near, small_send.at[0], small_recv.at[0], (here, beside))
    small_far = remote(product_sum, product_far, small_send.at[1], small_recv.at[1], (here, across))
    small_near.start()

    def launch(step, carry):
        j = (step + 1) % ep_count
        near(0, j).start()
        near(1, j).start()
        return carry

    lax.fori_loop(0, ep_count, launch, 0)
    small_near.wait_recv()
    product_sum[...] = product_ref[...] + product_near[...]
    small_far.start()

    def middle(step, carry):
        j = (step + 1) % ep_count
        near(0, j).wait_recv()
        target = (here + j) % ep_count
        mine = rows_ref[target, :, columns(across)].astype(jnp.float32)
        far_send[j] = (mine + near_buf[0, j].astype(jnp.float32)).astype(jnp.bfloat16)
        far(j).start()
        return carry

    lax.fori_loop(0, ep_count, middle, 0)
    small_far.wait_recv()
    product_send[...] = product_sum[...] + product_far[...]

    def total(j):
        near(1, j).wait_recv()
        far(j).wait_recv()
        target = (here + j) % ep_count
        mine = rows_ref[target, :, columns(part)].astype(jnp.float32)
        added = mine + near_buf[1, j].astype(jnp.float32) + far_buf[j].astype(jnp.float32)
        return added.astype(jnp.bfloat16)

    def end(j, carry):
        last_send[j] = total(j)
        last(j).start()
        last_product(j).start()
        return carry

    lax.fori_loop(1, ep_count, end, 0)
    back_ref[here] = total(0)
    back_product[here] = product_send[here]

    small_near.wait_send()
    small_far.wait_send()

    def finish(j, carry):
        near(0, j).wait_send()
        near(1, j).wait_send()
        far(j).wait_send()

        @pl.when(j >= 1)
        def _():
            last(j).wait()
            last_product(j).wait()

        return carry

    lax.fori_loop(0, ep_count, finish, 0)


def combine(rows, products, width):
    ep_count, capacity, _ = rows.shape
    one = (ep_count, capacity, width)
    small = pltpu.VMEM(products.shape, jnp.float32)
    dma = pltpu.SemaphoreType.DMA
    return pl.pallas_call(
        combine_kernel,
        out_shape=(
            jax.ShapeDtypeStruct(one, jnp.bfloat16),
            jax.ShapeDtypeStruct(products.shape, jnp.float32),
        ),
        in_specs=[pl.BlockSpec(memory_space=pltpu.VMEM)] * 2,
        out_specs=(pl.BlockSpec(memory_space=pltpu.VMEM),) * 2,
        scratch_shapes=[
            pltpu.VMEM((2,) + one, jnp.bfloat16),
            pltpu.VMEM(one, jnp.bfloat16),
            pltpu.VMEM(one, jnp.bfloat16),
            pltpu.VMEM(one, jnp.bfloat16),
            small, small, small, small,
            dma((2, ep_count)), dma((2, ep_count)),
            dma((ep_count,)), dma((ep_count,)), dma((ep_count,)), dma((ep_count,)),
            dma((ep_count,)), dma((ep_count,)), dma((2,)), dma((2,)),
        ],
        compiler_params=pltpu.CompilerParams(
            collective_id=1, has_side_effects=True, vmem_limit_bytes=48 * 1024 * 1024
        ),
    )(rows, products)


def local(tokens, routes, gate_weights, out_grad, w_gate, w_up, w_down):
    f32, bf16 = jnp.float32, jnp.bfloat16
    ep_count = lax.axis_size("ep")
    tp_count = lax.axis_size("tp")
    part = lax.axis_index("tp")
    token_count, model_width = tokens.shape
    top_count = routes.shape[1]
    experts = ep_count * w_gate.shape[0]
    capacity = token_count * top_count * 5 // (4 * experts)
    width = model_width // tp_count

    match = routes[:, :, None] == jnp.arange(experts, dtype=jnp.int32)[None, None, :]
    named = jnp.any(match, axis=1)
    before = jnp.arange(token_count)[:, None] > jnp.arange(token_count)[None, :]
    rank = jnp.dot(before.astype(bf16), named.astype(bf16), preferred_element_type=f32)
    rank = jnp.where(named, rank.astype(jnp.int32), -1)
    pick = rank.T[:, None, :] == jnp.arange(capacity, dtype=jnp.int32)[None, :, None]
    pick_flat = pick.reshape(experts * capacity, token_count).astype(bf16)
    weight_of = jnp.sum(jnp.where(match, gate_weights[:, :, None], 0.0), axis=1)
    send_weights = jnp.sum(jnp.where(pick, weight_of.T[:, None, :], 0.0), axis=2)
    sends = []
    for array in (tokens, out_grad):
        own = lax.dynamic_slice_in_dim(array, part * width, width, 1)
        picked = jnp.dot(pick_flat, own, preferred_element_type=f32).astype(bf16)
        sends.append(picked.reshape(experts, capacity, width))

    rows, grads, weights = dispatch(*sends, send_weights[:, None, :], model_width)
    row_count = ep_count * capacity
    x_rows = rows.reshape(row_count, model_width)
    dy_rows = grads.reshape(row_count, model_width)
    slot_weights = weights.reshape(row_count, 1)

    gate_pre = jnp.dot(x_rows, w_gate[0], preferred_element_type=f32)
    up_pre = jnp.dot(x_rows, w_up[0], preferred_element_type=f32)
    plain_grad = jnp.einsum("rd,fd->rf", dy_rows, w_down[0], preferred_element_type=f32)
    glu = jnp.minimum(gate_pre, clamp_limit)
    linear = jnp.clip(up_pre, -clamp_limit, clamp_limit)
    sigma = jax.nn.sigmoid(sigmoid_slope * glu)
    active = glu * sigma
    hidden = active * (linear + 1.0)
    product = jnp.sum(hidden * plain_grad, axis=1)
    hidden_grad = plain_grad * slot_weights
    slope_term = sigma + sigmoid_slope * active * (1.0 - sigma)
    gate_pre_grad = jnp.where(
        gate_pre < clamp_limit, hidden_grad * (linear + 1.0) * slope_term, 0.0
    ).astype(bf16)
    up_pre_grad = jnp.where(jnp.abs(up_pre) < clamp_limit, hidden_grad * active, 0.0).astype(bf16)
    hidden = (hidden * slot_weights).astype(bf16)

    row_term = jnp.einsum("rf,df->rd", gate_pre_grad, w_gate[0], preferred_element_type=f32)
    row_term = row_term + jnp.einsum(
        "rf,df->rd", up_pre_grad, w_up[0], preferred_element_type=f32
    )
    row_term = row_term.astype(bf16).reshape(ep_count, capacity, model_width)
    back_rows, back_products = combine(
        row_term, product.reshape(ep_count, 1, capacity), width
    )
    gate_grads = jnp.einsum("rd,rf->df", x_rows, gate_pre_grad, preferred_element_type=f32)
    up_grads = jnp.einsum("rd,rf->df", x_rows, up_pre_grad, preferred_element_type=f32)
    down_grads = jnp.einsum("rf,rd->fd", hidden, dy_rows, preferred_element_type=f32)
    token_grad = jnp.einsum(
        "rt,rw->tw", pick_flat, back_rows.reshape(row_count, width), preferred_element_type=f32
    ).astype(bf16)
    found = jnp.sum(jnp.where(pick, back_products.reshape(experts, capacity, 1), 0.0), axis=1)
    gate_grad = jnp.sum(jnp.where(match, found.T[:, None, :], 0.0), axis=2)
    return (token_grad, gate_grad, gate_grads[None], up_grads[None], down_grads[None])


def solution(mesh):
    return jax.shard_map(
        local,
        mesh=mesh,
        in_specs=(
            P("ep", None),
            P("ep", None),
            P("ep", None),
            P("ep", None),
            P("ep", None, "tp"),
            P("ep", None, "tp"),
            P("ep", "tp", None),
        ),
        out_specs=(
            P("ep", "tp"),
            P("ep", None),
            P("ep", None, "tp"),
            P("ep", None, "tp"),
            P("ep", "tp", None),
        ),
        check_vma=False,
    )
```

profile of v0, /device:TPU:0, one launch (start us, length us, event | category | flops | bytes accessed | tf_op | source)
XLA Modules:
  0.0 180.5 jit_solution(12372572740274645260)
XLA Ops:
  0.7 0.8 fusion.19
  1.4 0.2 fusion.4
  1.6 0.7 select_reduce_fusion.3
  2.3 0.3 select_reduce_fusion.1
  2.7 0.6 broadcast_in_dim.81.weight_ref
  3.3 0.1 eq.45
  3.4 0.2 bitcast_compare_fusion
  3.6 2.5 %convolution_convert_fusion = bf16[1280,512]{1,0:T(8,128)(2,1)} fusion(pred[1280,256]{1,0:T(32,128)(4,1)S(1)} %bitcast_compare_fusion, bf16[256,2048]{1,0:T(8,128)(2,1)} %param.10, s32[]{:T(128)S(6)} %select_n.33), kind=kOutput, calls=%fused_computation.1 | convolution fusion | flops 336199680 | bytes 1900548 | tf_op jit(solution)/shard_map/dot_general | solution.py:314
  6.2 2.5 %convolution_convert_fusion.1 = bf16[1280,512]{1,0:T(8,128)(2,1)} fusion(pred[1280,256]{1,0:T(32,128)(4,1)S(1)} %bitcast_compare_fusion, bf16[256,2048]{1,0:T(8,128)(2,1)} %param.7, s32[]{:T(128)S(6)} %select_n.33), kind=kOutput, calls=%fused_computation.2 | convolution fusion | flops 336199680 | bytes 1900548 | tf_op jit(solution)/shard_map/dot_general | solution.py:314
  8.7 81.4 %shard_map.110 = (bf16[8,160,2048]{2,1,0:T(8,128)(2,1)}, bf16[8,160,2048]{2,1,0:T(8,128)(2,1)}, f32[8,1,160]{2,1,0:T(1,128)}) custom-call(bf16[8,160,512]{2,1,0:T(8,128)(2,1)} %bitcast.53, bf16[8,160,512]{2,1,0:T(8,128)(2,1)} %bitcast.52, f32[8,1,160]{2,1,0:T(1,128)} %broadcast_in_dim.81.weight_ref), custom_call_target="tpu_custom_call" | custom-call | tf_op jit(solution)/shard_map/pallas_call | solution.py:149
  90.1 0.7 reduce
  90.9 4.2 %fusion.6 = f32[1280,256]{0,1:T(8,128)S(1)} fusion(bf16[1280,2048]{1,0:T(8,128)(2,1)} %bitcast.57, bf16[1,2048,256]{2,1,0:T(8,128)(2,1)S(1)} %copy-done.4), kind=kOutput, calls=%fused_computation.25 | convolution fusion | flops 1342177280 | bytes 7602176 | tf_op jit(solution)/shard_map/dot_general | solution.py:324
  95.2 1.7 fusion.12
  97.0 3.4 %multiply_reduce_fusion = (f32[1280]{0:T(1024)S(1)}, bf16[1280,256]{0,1:T(8,128)(2,1)}, f32[1280,256]{0,1:T(8,128)}) fusion(f32[1280,256]{0,1:T(8,128)S(1)} %fusion.6, f32[1280,256]{0,1:T(8,128)S(1)} %fusion.12, f32[1280]{0:T(1024)S(1)} %mul.48, bf16[1280,2048]{1,0:T(8,128)(2,1)S(1)} %bitcast.63, bf16[1,256,2048]{2,1,0:T(8,128)(2,1)S(1)} %copy-done.8), kind=kOutput, calls=%fused_computation.9 | convolution fusion | flops 1347746560 | bytes 10889216 | tf_op jit(solution)/shard_map/rd,fd->rf/dot_general | solution.py:325
  100.4 3.2 %convolution_bitcast_fusion = f32[1,256,2048]{2,1,0:T(8,128)} fusion(bf16[1280,2048]{1,0:T(8,128)(2,1)S(1)} %bitcast.64, f32[1280]{0:T(1024)S(1)} %mul.48, f32[1280,256]{0,1:T(8,128)S(1)} %fusion.6, f32[1280,256]{0,1:T(8,128)S(1)} %fusion.12), kind=kOutput, calls=%fused_computation.3 | convolution fusion | flops 1345781760 | bytes 9966592 | tf_op jit(solution)/shard_map/rf,rd->fd/dot_general | solution.py:350
  103.5 0.1 reshape.46.product_ref
  103.6 5.7 %convolution_bitcast_fusion.1 = f32[1,2048,256]{2,1,0:T(8,128)} fusion(bf16[1280,2048]{1,0:T(8,128)(2,1)} %bitcast.58, bf16[1280,256]{0,1:T(8,128)(2,1)} %get-tuple-element.16), kind=kOutput, calls=%fused_computation.4 | convolution fusion | flops 1342177280 | bytes 7995392 | tf_op jit(solution)/shard_map/rd,rf->df/dot_general | solution.py:349
  109.3 5.7 %convolution_bitcast_fusion.2 = f32[1,2048,256]{2,1,0:T(8,128)} fusion(bf16[1280,2048]{1,0:T(8,128)(2,1)} %bitcast.59, f32[1280,256]{0,1:T(8,128)S(1)} %copy-done.2, f32[1280,256]{0,1:T(8,128)S(1)} %copy-done.3, f32[1280,256]{0,1:T(8,128)S(1)} %fusion.6, f32[1280]{0:T(1024)S(1)} %mul.48), kind=kOutput, calls=%fused_computation.5 | convolution fusion | flops 1348075520 | bytes 11277312 | tf_op jit(solution)/shard_map/rd,rf->df/dot_general | solution.py:348
  115.0 2.4 %fusion.10 = f32[1280,2048]{1,0:T(8,128)S(1)} fusion(bf16[1,2048,256]{2,1,0:T(8,128)(2,1)S(1)} %copy-done, f32[1280,256]{0,1:T(8,128)S(1)} %copy-done.2, f32[1280,256]{0,1:T(8,128)S(1)} %copy-done.3, f32[1280,256]{0,1:T(8,128)S(1)} %fusion.6, f32[1280]{0:T(1024)S(1)} %mul.48), kind=kOutput, calls=%fused_computation.29 | convolution fusion | flops 1348075520 | bytes 15471616 | tf_op jit(solution)/shard_map/rf,df->rd/dot_general | solution.py:340
  117.5 3.9 %add_convert_fusion = bf16[1280,2048]{1,0:T(8,128)(2,1)} fusion(f32[1280,2048]{1,0:T(8,128)S(1)} %fusion.10, bf16[1280,256]{0,1:T(8,128)(2,1)S(1)} %copy-done.5, bf16[1,2048,256]{2,1,0:T(8,128)(2,1)S(1)} %copy-done.4), kind=kOutput, calls=%fused_computation | convolution fusion | flops 1347420160 | bytes 17432576 | tf_op jit(solution)/shard_map/rf,df->rd/dot_general | solution.py:341
  121.4 56.9 %shard_map.111 = (bf16[8,160,512]{2,1,0:T(8,128)(2,1)S(1)}, f32[8,1,160]{2,1,0:T(1,128)S(1)}) custom-call(bf16[8,160,2048]{2,1,0:T(8,128)(2,1)} %bitcast.51, f32[8,1,160]{2,1,0:T(1,128)S(1)} %reshape.46.product_ref), custom_call_target="tpu_custom_call" | custom-call | tf_op jit(solution)/shard_map/pallas_call | solution.py:267
  178.3 1.3 fusion.2
  179.6 0.2 select_reduce_fusion
  179.9 0.6 select_reduce_fusion.2
  (26 shorter events, 0.2 us)
Async XLA Ops:
  0.6 94.5 %copy-start = (bf16[1,2048,256]{2,1,0:T(8,128)(2,1)S(1)}, bf16[1,2048,256]{2,1,0:T(8,128)(2,1)}, u32[]{:S(2)}) copy-start(bf16[1,2048,256]{2,1,0:T(8,128)(2,1)} %param.11) | copy-start | bytes 3145732
  8.7 82.2 %copy-start.4 = (bf16[1,2048,256]{2,1,0:T(8,128)(2,1)S(1)}, bf16[1,2048,256]{2,1,0:T(8,128)(2,1)}, u32[]{:S(2)}) copy-start(bf16[1,2048,256]{2,1,0:T(8,128)(2,1)} %param.12) | copy-start | bytes 3145732
  90.9 4.3 %copy-start.7 = (bf16[8,160,2048]{2,1,0:T(8,128)(2,1)S(1)}, bf16[8,160,2048]{2,1,0:T(8,128)(2,1)}, u32[]{:S(2)}) copy-start(bf16[8,160,2048]{2,1,0:T(8,128)(2,1)} %get-tuple-element.10) | copy-start | bytes 15728644
  90.9 6.0 %slice-start = ((s8[5242880]{0:T(1024)(128)(4,1)}), s8[4194304]{0:T(1024)(128)(4,1)S(1)}, s32[]{:S(2)}) async-start(s8[5242880]{0:T(1024)(128)(4,1)} %bitcast.61), calls=%async_computation | async-start | bytes 8388608
  95.2 1.7 slice-start.1
  95.2 1.8 copy-start.8
  97.0 3.4 %copy-start.1 = (f32[1280,256]{0,1:T(8,128)}, f32[1280,256]{0,1:T(8,128)S(1)}, u32[]{:S(2)}) copy-start(f32[1280,256]{0,1:T(8,128)S(1)} %fusion.12) | copy-start | bytes 3932164
  103.6 5.7 %copy-start.2 = (f32[1280,256]{0,1:T(8,128)S(1)}, f32[1280,256]{0,1:T(8,128)}, u32[]{:S(2)}) copy-start(f32[1280,256]{0,1:T(8,128)} %copy-done.1) | copy-start | bytes 3932164
  103.6 5.7 %copy-start.3 = (f32[1280,256]{0,1:T(8,128)S(1)}, f32[1280,256]{0,1:T(8,128)}, u32[]{:S(2)}) copy-start(f32[1280,256]{0,1:T(8,128)} %get-tuple-element.17) | copy-start | bytes 3932164
  115.0 2.4 %copy-start.5 = (bf16[1280,256]{0,1:T(8,128)(2,1)S(1)}, bf16[1280,256]{0,1:T(8,128)(2,1)}, u32[]{:S(2)}) copy-start(bf16[1280,256]{0,1:T(8,128)(2,1)} %get-tuple-element.16) | copy-start | bytes 1966084
  178.3 1.5 copy-start.6
where the time goes:
time: 182 us; the launch traced here: 180 us
  Pallas kernels  138 us (76%)
  matrix products  36.7 us (20%)
  other arithmetic  3.71 us (2%)
    pallas_call x1, Pallas kernels, dispatch(): pl.pallas_call(dispatch_kernel, out_shape=(whole, whole, jax.ShapeDtypeSt...  81.4 us
    pallas_call x1, Pallas kernels, combine(): pl.pallas_call(combine_kernel, out_shape=(jax.ShapeDtypeStruct(one, jnp.b...  56.9 us
    dot_general x1, matrix products, local(): jnp.einsum('rd,rf->df', x_rows, up_pre_grad, preferred_element_type=f32)  5.72 us
    dot_general x1, matrix products, local(): jnp.einsum('rd,rf->df', x_rows, gate_pre_grad, preferred_element_type=f32)  5.71 us
    dot_general x2, matrix products, local(): picked = jnp.dot(pick_flat, own, preferred_element_type=f32).astype(bf16)  5.05 us
    dot_general x1, matrix products, local(): up_pre = jnp.dot(x_rows, w_up[0], preferred_element_type=f32)  4.24 us
    dot_general x1, matrix products, local(): jnp.einsum('rf,df->rd', up_pre_grad, w_up[0], preferred_element_type=f32)  3.93 us

commit v1 on v0

--- a/solution.py
+++ b/solution.py
@@ -356,9 +356,476 @@
     return (token_grad, gate_grad, gate_grads[None], up_grads[None], down_grads[None])
 
 
+def fused_kernel(
+    tok_ref, grd_ref, meta_ref, gate_ref, up_ref, down_ref,
+    token_out, found_out, gate_out, up_out, down_out,
+    line, metas, pick_send, rows, gate_g, up_g, hid,
+    near_send, near_buf, mine, own_sum, back_send, back_buf,
+    z_send, z_buf, total, y_send, y_buf,
+    found_loc, found_near, found_sum, found_far, found_send,
+    chain_s, chain_r, xm_s, xm_r, x_s, x_r, n_s, n_r, f_s, f_r, o_s, o_r,
+    c_s, c_r, b_s, b_r, z_s, z_r, y_s, y_r, sm_s, sm_r, l_s, l_r,
+):
+    f32, bf16 = jnp.float32, jnp.bfloat16
+    ep_count, here, part, beside, across = partners()
+    count = ep_count // 2
+    z, x = here // 2, here % 2
+    other = here + 1 - 2 * x
+    plane, core = part // 2, part % 2
+    capacity = rows.shape[2]
+    model_width = tok_ref.shape[1]
+    width = token_out.shape[1]
+    token_count = tok_ref.shape[0]
+
+    def columns(owner):
+        return pl.ds(pl.multiple_of(owner * width, width), width)
+
+    def order(i):
+        high = (2 * z) // count
+        paired = z * (1 - high) + (count - 1 - z) * high
+        inside = (2 * paired + 4 * count - i) // (4 * count)
+        step = z + ((i + 1) // 2) * (1 - 2 * (i % 2))
+        rest = i * (1 - high) + (count - 1 - i) * high
+        return inside * step + (1 - inside) * rest
+
+    def chain(kind, zi, way):
+        ref = metas.at[2 * zi + x] if kind == 2 else line.at[kind, zi]
+        to = here + 2 - 4 * way
+        return remote(ref, ref, chain_s.at[way, kind, zi], chain_r.at[kind, zi], (to, part))
+
+    def cross_meta(zi):
+        ref = metas.at[2 * zi + x]
+        return remote(ref, ref, xm_s.at[zi], xm_r.at[zi], (other, part))
+
+    def cross(kind, zi):
+        return remote(
+            pick_send.at[kind, zi], rows.at[kind, 2 * zi + x, :, columns(part)],
+            x_s.at[kind, zi], x_r.at[kind, zi], (other, part),
+        )
+
+    def forward(kind, source, owner, sent, got, to):
+        ref = rows.at[kind, source, :, columns(owner)]
+        return remote(ref, ref, sent.at[kind, source], got.at[kind, source], (here, to))
+
+    def near(kind, source):
+        return forward(kind, source, part, n_s, n_r, beside)
+
+    def far(kind, source):
+        return forward(kind, source, part, f_s, f_r, across)
+
+    def onward(kind, source):
+        return forward(kind, source, across, o_s, o_r, beside)
+
+    def pair(source):
+        return remote(
+            near_send.at[source], near_buf.at[source], c_s.at[source], c_r.at[source],
+            (here, beside),
+        )
+
+    def cross_back(zi):
+        return remote(back_send.at[zi], back_buf.at[zi], b_s.at[zi], b_r.at[zi], (other, part))
+
+    def line_back(zi):
+        return remote(z_send.at[zi], z_buf.at[z], z_s.at[zi], z_r.at[z], (2 * zi + x, part))
+
+    def line_got(zi):
+        return remote(z_send.at[zi], z_buf.at[zi], z_s.at[zi], z_r.at[zi], (2 * zi + x, part))
+
+    last_y = remote(y_send, y_buf, y_s.at[0], y_r.at[0], (here, across))
+    small_near = remote(found_loc, found_near, sm_s.at[0], sm_r.at[0], (here, beside))
+    small_far = remote(found_sum, found_far, sm_s.at[1], sm_r.at[1], (here, across))
+
+    def last_found(j):
+        peer = (here + j) % ep_count
+        return remote(found_send.at[peer], found_out.at[here], l_s.at[j], l_r.at[j], (peer, part))
+
+    slots = lax.broadcasted_iota(jnp.int32, (capacity, token_count), 0).astype(f32)
+
+    def matches(source, expert):
+        return slots == metas[source, pl.ds(expert, 1), :]
+
+    def pick(source, expert):
+        return jnp.where(matches(source, expert), 1.0, 0.0).astype(bf16)
+
+    line[0, z] = tok_ref[:, columns(part)]
+    line[1, z] = grd_ref[:, columns(part)]
+    metas[here] = meta_ref[...]
+    greet(ep_count, here, part, beside, across)
+
+    @pl.when(z < count - 1)
+    def _():
+        for kind in (2, 0, 1):
+            chain(kind, z, 0).start()
+
+    @pl.when(z > 0)
+    def _():
+        for kind in (2, 0, 1):
+            chain(kind, z, 1).start()
+
+    def take(kind, zi):
+        chain(kind, zi, 0).wait_recv()
+
+        @pl.when((zi < z) & (z < count - 1))
+        def _():
+            chain(kind, zi, 0).start()
+
+        @pl.when((zi > z) & (z > 0))
+        def _():
+            chain(kind, zi, 1).start()
+
+    def gather(i):
+        zi = order(i)
+        source = 2 * zi + x
+
+        @pl.when(i >= 1)
+        def _():
+            take(2, zi)
+
+        cross_meta(zi).start()
+        for kind in range(2):
+            @pl.when(i >= 1)
+            def _():
+                take(kind, zi)
+
+            picked = jnp.dot(
+                pick(source, other), line[kind, zi], preferred_element_type=f32
+            )
+            pick_send[kind, zi] = picked.astype(bf16)
+            cross(kind, zi).start()
+
+            @pl.when(i >= 1)
+            def _():
+                own = jnp.dot(pick(source, here), line[kind, zi], preferred_element_type=f32)
+                rows[kind, source, :, columns(part)] = own.astype(bf16)
+                far(kind, source).start()
+                near(kind, source).start()
+
+            @pl.when(i == 0)
+            def _():
+                whole = grd_ref if kind else tok_ref
+                for q in range(model_width // width):
+                    at = pl.ds(q * width, width)
+                    own = jnp.dot(
+                        pick(source, here), whole[:, at], preferred_element_type=f32
+                    )
+                    rows[kind, source, :, at] = own.astype(bf16)
+
+    def arrive(i):
+        zi = order(i)
+        for kind in range(2):
+            cross(kind, zi).wait_recv()
+            far(kind, 2 * zi + 1 - x).start()
+            near(kind, 2 * zi + 1 - x).start()
+        cross_meta(zi).wait_recv()
+
+    def hand_on(source):
+        for kind in range(2):
+            far(kind, source).wait_recv()
+            onward(kind, source).start()
+
+    def compute(source, local_rows):
+        @pl.when(local_rows == 0)
+        def _():
+            for kind in range(2):
+                near(kind, source).wait_recv()
+                onward(kind, source).wait_recv()
+
+        nt = (((1,), (1,)), ((), ()))
+        x_rows = rows[0, source]
+        gate_pre = jnp.dot(x_rows, gate_ref[...], preferred_element_type=f32)
+        up_pre = jnp.dot(x_rows, up_ref[...], preferred_element_type=f32)
+        plain = lax.dot_general(rows[1, source], down_ref[...], nt, preferred_element_type=f32)
+        hit = matches(source, here)
+        weight_row = metas[source, pl.ds(here + ep_count, 1), :]
+        weight = jnp.sum(jnp.where(hit, weight_row, 0.0), axis=1, keepdims=True)
+        glu = jnp.minimum(gate_pre, clamp_limit)
+        linear = jnp.clip(up_pre, -clamp_limit, clamp_limit)
+        sigma = jax.nn.sigmoid(sigmoid_slope * glu)
+        active = glu * sigma
+        hidden = active * (linear + 1.0)
+        product = jnp.sum(hidden * plain, axis=1, keepdims=True)
+        found_loc[source] = jnp.sum(jnp.where(hit, product, 0.0), axis=0, keepdims=True)
+        hidden_grad = plain * weight
+        slope_term = sigma + sigmoid_slope * active * (1.0 - sigma)
+        gate_grad = jnp.where(
+            gate_pre < clamp_limit, hidden_grad * (linear + 1.0) * slope_term, 0.0
+        ).astype(bf16)
+        up_grad = jnp.where(jnp.abs(up_pre) < clamp_limit, hidden_grad * active, 0.0).astype(bf16)
+        gate_g[source] = gate_grad
+        up_g[source] = up_grad
+        hid[source] = (hidden * weight).astype(bf16)
+        for own in range(2):
+            for half in range(2):
+                owner = 2 * half + (core if own else 1 - core)
+                term = lax.dot_general(
+                    gate_g[source], gate_ref[columns(owner), :], nt, preferred_element_type=f32
+                ) + lax.dot_general(
+                    up_g[source], up_ref[columns(owner), :], nt, preferred_element_type=f32
+                )
+                at = pl.ds(half * width, width)
+                if own:
+                    mine[source, :, at] = term.astype(bf16)
+                else:
+                    near_send[source, :, at] = term.astype(bf16)
+            if not own:
+                pair(source).start()
+
+    def pair_sum(source):
+        pair(source).wait_recv()
+        added = mine[source].astype(f32) + near_buf[source].astype(f32)
+        return added.astype(bf16)
+
+    def merge(i):
+        zi = order(i)
+        source = 2 * zi + x
+        cross_back(zi).wait_recv()
+        tn = (((0,), (0,)), ((), ()))
+        own_pick, other_pick = pick(source, here), pick(source, other)
+        for half in range(2):
+            at = pl.ds(half * width, width)
+            added = lax.dot_general(
+                own_pick, own_sum[zi, :, at], tn, preferred_element_type=f32
+            ) + lax.dot_general(
+                other_pick, back_buf[zi, :, at], tn, preferred_element_type=f32
+            )
+
+            @pl.when(i == 0)
+            def _():
+                total[:, at] = added
+
+            @pl.when(i >= 1)
+            def _():
+                z_send[zi, :, at] = added.astype(bf16)
+
+        @pl.when(i >= 1)
+        def _():
+            line_back(zi).start()
+
+    def body(i, carry):
+        @pl.when(i < count)
+        def _():
+            gather(i)
+
+        @pl.when((i >= 2) & (i <= count))
+        def _():
+            hand_on(2 * order(i - 1) + x)
+
+        @pl.when(i >= 2)
+        def _():
+            compute(2 * order(i - 2) + 1 - x, 0)
+            own_sum[order(i - 2)] = pair_sum(2 * order(i - 2) + x)
+
+        @pl.when(i < count)
+        def _():
+            arrive(i)
+
+        @pl.when((i >= 1) & (i <= count))
+        def _():
+            hand_on(2 * order(i - 1) + 1 - x)
+            compute(2 * order(i - 1) + x, (count - i + 1) // count)
+
+        @pl.when(i >= 2)
+        def _():
+            zi = order(i - 2)
+            back_send[zi] = pair_sum(2 * zi + 1 - x)
+            cross_back(zi).start()
+
+        @pl.when(i >= 3)
+        def _():
+            merge(i - 3)
+
+        return carry
+
+    lax.fori_loop(0, count + 2, body, 0)
+    small_near.start()
+
+    def weights(n, carry):
+        chunk = 256
+        tn = (((0,), (0,)), ((), ()))
+        at = pl.ds(pl.multiple_of(n * chunk, chunk), chunk)
+        flat = ep_count * capacity
+        x_part = rows[0, :, :, at].reshape(flat, chunk)
+        g_part = rows[1, :, :, at].reshape(flat, chunk)
+        units = gate_g.shape[2]
+        gate_out[at, :] = lax.dot_general(
+            x_part, gate_g[...].reshape(flat, units), tn, preferred_element_type=f32
+        )
+        up_out[at, :] = lax.dot_general(
+            x_part, up_g[...].reshape(flat, units), tn, preferred_element_type=f32
+        )
+        down_out[:, at] = lax.dot_general(
+            hid[...].reshape(flat, units), g_part, tn, preferred_element_type=f32
+        )
+        return carry
+
+    chunks = model_width // 256
+    small_near.wait_recv()
+    found_sum[...] = found_loc[...] + found_near[...]
+    small_far.start()
+    lax.fori_loop(0, chunks // 2, weights, 0)
+    small_far.wait_recv()
+    found_send[...] = found_sum[...] + found_far[...]
+    found_out[here] = found_send[here]
+
+    def share(j, carry):
+        last_found(j).start()
+        return carry
+
+    lax.fori_loop(1, ep_count, share, 0)
+    merge(count - 1)
+    lax.fori_loop(chunks // 2, chunks, weights, 0)
+
+    def add(i, carry):
+        zi = order(i)
+        line_got(zi).wait_recv()
+        total[...] = total[...] + z_buf[zi].astype(f32)
+        return carry
+
+    lax.fori_loop(1, count, add, 0)
+    y_send[...] = total[:, columns(1 - plane)].astype(bf16)
+    last_y.start()
+    last_y.wait_recv()
+    token_out[...] = (total[:, columns(plane)] + y_buf[...].astype(f32)).astype(bf16)
+
+    def finish(zi, carry):
+        for kind in range(3):
+            @pl.when((zi <= z) & (z < count - 1))
+            def _():
+                chain(kind, zi, 0).wait_send()
+
+            @pl.when((zi >= z) & (z > 0))
+            def _():
+                chain(kind, zi, 1).wait_send()
+
+        cross_meta(zi).wait_send()
+        cross_back(zi).wait_send()
+        for kind in range(2):
+            cross(kind, zi).wait_send()
+
+        @pl.when((zi < z) | (zi > z))
+        def _():
+            line_back(zi).wait_send()
+
+        return carry
+
+    lax.fori_loop(0, count, finish, 0)
+
+    def finish_source(source, carry):
+        pair(source).wait_send()
+
+        @pl.when((source < here) | (source > here))
+        def _():
+            for kind in range(2):
+                near(kind, source).wait_send()
+                far(kind, source).wait_send()
+                onward(kind, source).wait_send()
+
+        return carry
+
+    lax.fori_loop(0, ep_count, finish_source, 0)
+
+    def finish_found(j, carry):
+        last_found(j).wait()
+        return carry
+
+    lax.fori_loop(1, ep_count, finish_found, 0)
+    last_y.wait_send()
+    small_near.wait_send()
+    small_far.wait_send()
+
+
+def fused(tokens, grads, meta, w_gate, w_up, w_down, capacity, width):
+    f32, bf16 = jnp.float32, jnp.bfloat16
+    ep_count = lax.axis_size("ep")
+    count = ep_count // 2
+    token_count, model_width = tokens.shape
+    units = w_gate.shape[1]
+    vm = pltpu.VMEM
+    dma = pltpu.SemaphoreType.DMA
+    small = vm((ep_count, 1, token_count), f32)
+    half = (capacity, 2 * width)
+    scratch = [
+        vm((2, count, token_count, width), bf16),
+        vm((ep_count,) + meta.shape, f32),
+        vm((2, count, capacity, width), bf16),
+        vm((2, ep_count, capacity, model_width), bf16),
+        vm((ep_count, capacity, units), bf16),
+        vm((ep_count, capacity, units), bf16),
+        vm((ep_count, capacity, units), bf16),
+        vm((ep_count,) + half, bf16),
+        vm((ep_count,) + half, bf16),
+        vm((ep_count,) + half, bf16),
+        vm((count,) + half, bf16),
+        vm((count,) + half, bf16),
+        vm((count,) + half, bf16),
+        vm((count, token_count, 2 * width), bf16),
+        vm((count, token_count, 2 * width), bf16),
+        vm((token_count, 2 * width), f32),
+        vm((token_count, width), bf16),
+        vm((token_count, width), bf16),
+        small, small, small, small, small,
+        dma((2, 3, count)), dma((3, count)),
+        dma((count,)), dma((count,)),
+        dma((2, count)), dma((2, count)),
+        dma((2, ep_count)), dma((2, ep_count)),
+        dma((2, ep_count)), dma((2, ep_count)),
+        dma((2, ep_count)), dma((2, ep_count)),
+        dma((ep_count,)), dma((ep_count,)),
+        dma((count,)), dma((count,)),
+        dma((count,)), dma((count,)),
+        dma((1,)), dma((1,)), dma((2,)), dma((2,)),
+        dma((ep_count,)), dma((ep_count,)),
+    ]
+    return pl.pallas_call(
+        fused_kernel,
+        out_shape=(
+            jax.ShapeDtypeStruct((token_count, width), bf16),
+            jax.ShapeDtypeStruct((ep_count, 1, token_count), f32),
+            jax.ShapeDtypeStruct((model_width, units), f32),
+            jax.ShapeDtypeStruct((model_width, units), f32),
+            jax.ShapeDtypeStruct((units, model_width), f32),
+        ),
+        in_specs=[pl.BlockSpec(memory_space=pltpu.VMEM)] * 6,
+        out_specs=(pl.BlockSpec(memory_space=pltpu.VMEM),) * 5,
+        scratch_shapes=scratch,
+        compiler_params=pltpu.CompilerParams(
+            collective_id=2, has_side_effects=True, vmem_limit_bytes=60 * 1024 * 1024
+        ),
+    )(tokens, grads, meta, w_gate, w_up, w_down)
+
+
+def gathered(tokens, routes, gate_weights, out_grad, w_gate, w_up, w_down):
+    f32, bf16 = jnp.float32, jnp.bfloat16
+    ep_count = lax.axis_size("ep")
+    token_count, model_width = tokens.shape
+    capacity = token_count * routes.shape[1] * 5 // (4 * ep_count)
+    width = model_width // lax.axis_size("tp")
+    by_expert = routes.T
+    match = by_expert[None, :, :] == jnp.arange(ep_count, dtype=jnp.int32)[:, None, None]
+    named = jnp.any(match, axis=1)
+    before = jnp.arange(token_count)[:, None] < jnp.arange(token_count)[None, :]
+    rank = jnp.dot(named.astype(bf16), before.astype(bf16), preferred_element_type=f32)
+    rank = jnp.where(named, rank, -1.0)
+    weight_of = jnp.sum(jnp.where(match, gate_weights.T[None, :, :], 0.0), axis=1)
+    meta = jnp.concatenate([rank, weight_of], axis=0)
+    token_grad, found, gate_grads, up_grads, down_grads = fused(
+        tokens, out_grad, meta, w_gate[0], w_up[0], w_down[0], capacity, width
+    )
+    gate_grad = jnp.sum(jnp.where(match, found, 0.0), axis=0).T
+    return (token_grad, gate_grad, gate_grads[None], up_grads[None], down_grads[None])
+
+
+def chosen(*args):
+    tokens, w_gate = args[0], args[4]
+    block_bytes = lax.axis_size("ep") * tokens.size * 2
+    if block_bytes <= 16 * 1024 * 1024 and w_gate.shape[0] == 1:
+        return gathered(*args)
+    return local(*args)
+
+
 def solution(mesh):
     return jax.shard_map(
-        local,
+        chosen,
         mesh=mesh,
         in_specs=(
             P("ep", None),

time: 182 us -> 142 us (0.78)
  matrix products: 36.7 us -> 0.15 us
  Pallas kernels: 138 us -> 127 us
  local copies, waits for them, and re-layouts: 0.95 us -> 9.23 us
    dot_general x12 -> x1, matrix products: 36.7 us -> 0.15 us  [gathered(): jnp.dot(named.astype(bf16), before.astype(bf16), preferred_element_type=f32)]
    pallas_call x2 -> x1, Pallas kernels: 138 us -> 127 us  [fused(): pl.pallas_call(fused_kernel, out_shape=(jax.ShapeDtypeStruct((token_count...]
    unnamed x23 -> x11, local copies, waits for them, and re-layouts: 0.1 us -> 9.23 us
where the time goes in v1:
time: 142 us; the launch traced here: 139 us
  Pallas kernels  127 us (89%)
  local copies, waits for them, and re-layouts  9.23 us (6%)
  other arithmetic  2.64 us (2%)
    pallas_call x1, Pallas kernels, fused(): pl.pallas_call(fused_kernel, out_shape=(jax.ShapeDtypeStruct((token_count...  127 us
    unnamed x11, local copies, waits for them, and re-layouts  9.23 us

profile of v1, /device:TPU:0, one launch (start us, length us, event | category | flops | bytes accessed | tf_op | source)
XLA Modules:
  0.0 139.4 jit_solution(8894526347526763300)
XLA Ops:
  0.6 0.7 fusion
  1.3 0.1 convolution_select_fusion
  1.5 0.7 select_reduce_fusion.1
  2.2 0.6 pad_maximum_fusion.meta_ref
  2.8 0.0 copy-start.2
  2.8 126.7 %shard_map.110 = (bf16[256,512]{1,0:T(8,128)(2,1)}, f32[8,1,256]{2,1,0:T(1,128)}, f32[2048,256]{1,0:T(8,128)}, f32[2048,256]{1,0:T(8,128)}, f32[256,2048]{1,0:T(8,128)}) custom-call(bf16[256,2048]{1,0:T(8,128)(2,1)} %tok_ref.1, bf16[256,2048]{1,0:T(8,128)(2,1)} %grd_ref.1, f32[16,256]{1,0:T(8,128)} %pad_maximum_fusion.meta_ref, bf16[2048,256]{1,0:T(8,128)(2,1)} %bitcast.16, ...), custom_call_target="tpu_custom_call" | custom-call | tf_op jit(solution)/shard_map/pallas_call | solution.py:779
  129.6 0.7 copy.14
  130.3 0.0 copy-done.2
  130.3 0.6 select_reduce_fusion
  130.9 1.7 %copy.19 = bf16[256,512]{1,0:T(8,128)(2,1)} copy(bf16[256,512]{1,0:T(8,128)(2,1)} %get-tuple-element.20) | data formatting | bytes 524288
  132.5 0.0 copy-start.1
  132.5 3.2 %copy.20 = f32[1,2048,256]{2,1,0:T(8,128)} copy(f32[1,2048,256]{2,1,0:T(8,128)} %bitcast.15) | data formatting | bytes 4194304
  135.7 0.0 copy-done.1
  135.7 0.0 copy-start
  135.7 1.3 copy.21
  137.1 1.0 copy-done
  138.1 1.3 copy.22
Async XLA Ops:
  2.8 127.5 %copy-start.2 = (s32[256,4]{0,1:T(4,128)S(1)}, s32[256,4]{0,1:T(4,128)}, u32[]{:S(2)}) copy-start(s32[256,4]{0,1:T(4,128)} %param.8) | copy-start | bytes 12292
  132.5 3.2 %copy-start.1 = (f32[2048,256]{1,0:T(8,128)S(1)}, f32[2048,256]{1,0:T(8,128)}, u32[]{:S(2)}) copy-start(f32[2048,256]{1,0:T(8,128)} %get-tuple-element.13) | copy-start | bytes 6291460
  135.7 2.3 %copy-start = (f32[256,2048]{1,0:T(8,128)S(1)}, f32[256,2048]{1,0:T(8,128)}, u32[]{:S(2)}) copy-start(f32[256,2048]{1,0:T(8,128)} %get-tuple-element.14) | copy-start | bytes 6291460

commit v2 on v1

--- a/solution.py
+++ b/solution.py
@@ -8,6 +8,7 @@
 clamp_limit = 7.0
 sigmoid_slope = 1.702
 MESH = pl.DeviceIdType.MESH
+far_step = 2
 
 
 def partners():
@@ -357,14 +358,14 @@
 
 
 def fused_kernel(
-    tok_ref, grd_ref, meta_ref, gate_ref, up_ref, down_ref,
+    tok_hbm, grd_hbm, route_hbm, share_hbm, gate_hbm, up_hbm, down_hbm,
     token_out, found_out, gate_out, up_out, down_out,
-    line, metas, pick_send, rows, gate_g, up_g, hid,
+    tok_ref, grd_ref, route_ref, share_ref, gate_ref, up_ref, down_ref, line, metas, pick_send, pick_extra, rows, gate_g, up_g, hid,
     near_send, near_buf, mine, own_sum, back_send, back_buf,
-    z_send, z_buf, total, y_send, y_buf,
+    half_send, half_buf, z_send, z_buf, total, total_half, y_send, y_buf,
     found_loc, found_near, found_sum, found_far, found_send,
-    chain_s, chain_r, xm_s, xm_r, x_s, x_r, n_s, n_r, f_s, f_r, o_s, o_r,
-    c_s, c_r, b_s, b_r, z_s, z_r, y_s, y_r, sm_s, sm_r, l_s, l_r,
+    chain_s, chain_r, xm_s, xm_r, x_s, x_r, e_s, e_r, n_s, n_r, f_s, f_r, o_s, o_r,
+    c_s, c_r, h_s, h_r, b_s, b_r, z_s, z_r, y_s, y_r, sm_s, sm_r, l_s, l_r, in_s,
 ):
     f32, bf16 = jnp.float32, jnp.bfloat16
     ep_count, here, part, beside, across = partners()
@@ -381,12 +382,11 @@
         return pl.ds(pl.multiple_of(owner * width, width), width)
 
     def order(i):
-        high = (2 * z) // count
-        paired = z * (1 - high) + (count - 1 - z) * high
-        inside = (2 * paired + 4 * count - i) // (4 * count)
-        step = z + ((i + 1) // 2) * (1 - 2 * (i % 2))
-        rest = i * (1 - high) + (count - 1 - i) * high
-        return inside * step + (1 - inside) * rest
+        mixed, bit = 0, 1
+        while bit < count:
+            mixed = mixed + ((z // bit + i // bit) % 2) * bit
+            bit = 2 * bit
+        return mixed
 
     def chain(kind, zi, way):
         ref = metas.at[2 * zi + x] if kind == 2 else line.at[kind, zi]
@@ -403,6 +403,12 @@
             x_s.at[kind, zi], x_r.at[kind, zi], (other, part),
         )
 
+    def cross_extra():
+        return remote(
+            pick_extra, rows.at[1, here, :, columns(across)],
+            e_s.at[0], e_r.at[0], (other, part),
+        )
+
     def forward(kind, source, owner, sent, got, to):
         ref = rows.at[kind, source, :, columns(owner)]
         return remote(ref, ref, sent.at[kind, source], got.at[kind, source], (here, to))
@@ -422,14 +428,44 @@
             (here, beside),
         )
 
-    def cross_back(zi):
-        return remote(back_send.at[zi], back_buf.at[zi], b_s.at[zi], b_r.at[zi], (other, part))
-
-    def line_back(zi):
-        return remote(z_send.at[zi], z_buf.at[z], z_s.at[zi], z_r.at[z], (2 * zi + x, part))
-
-    def line_got(zi):
-        return remote(z_send.at[zi], z_buf.at[zi], z_s.at[zi], z_r.at[zi], (2 * zi + x, part))
+    def half_over(source):
+        return remote(
+            half_send.at[source], half_buf.at[source], h_s.at[source], h_r.at[source],
+            (here, across),
+        )
+
+    def is_far(zi):
+        return order(zi) >= far_step
+
+    def cut(ref, zi, small):
+        return ref.at[zi, :, pl.ds(0, width)] if small else ref.at[zi]
+
+    def cross_back(zi, small):
+        return remote(
+            cut(back_send, zi, small), cut(back_buf, zi, small),
+            b_s.at[zi], b_r.at[zi], (other, part),
+        )
+
+    def line_back(zi, small):
+        return remote(
+            cut(z_send, zi, small), cut(z_buf, z, small),
+            z_s.at[zi], z_r.at[z], (2 * zi + x, part),
+        )
+
+    def line_got(zi, small):
+        return remote(
+            cut(z_send, zi, small), cut(z_buf, zi, small),
+            z_s.at[zi], z_r.at[zi], (2 * zi + x, part),
+        )
+
+    def either(zi, act):
+        @pl.when(is_far(zi))
+        def _():
+            act(True)
+
+        @pl.when(jnp.logical_not(is_far(zi)))
+        def _():
+            act(False)
 
     last_y = remote(y_send, y_buf, y_s.at[0], y_r.at[0], (here, across))
     small_near = remote(found_loc, found_near, sm_s.at[0], sm_r.at[0], (here, beside))
@@ -447,10 +483,47 @@
     def pick(source, expert):
         return jnp.where(matches(source, expert), 1.0, 0.0).astype(bf16)
 
-    line[0, z] = tok_ref[:, columns(part)]
-    line[1, z] = grd_ref[:, columns(part)]
-    metas[here] = meta_ref[...]
-    greet(ep_count, here, part, beside, across)
+    barrier = pltpu.get_barrier_semaphore()
+    pl.semaphore_signal(barrier, inc=1, device_id=(here, beside), device_id_type=MESH)
+    pl.semaphore_signal(barrier, inc=1, device_id=(here, across), device_id_type=MESH)
+
+    def hail(j, carry):
+        peer = (here + j) % ep_count
+        pl.semaphore_signal(barrier, inc=1, device_id=(peer, part), device_id_type=MESH)
+        return carry
+
+    lax.fori_loop(1, ep_count, hail, 0)
+    loads = [
+        pltpu.make_async_copy(src, dst, in_s.at[n])
+        for n, (src, dst) in enumerate((
+            (route_hbm, route_ref), (share_hbm, share_ref),
+            (tok_hbm.at[:, columns(part)], line.at[0, z]),
+            (grd_hbm.at[:, columns(part)], line.at[1, z]),
+            (tok_hbm, tok_ref), (grd_hbm, grd_ref),
+            (gate_hbm, gate_ref), (up_hbm, up_ref), (down_hbm, down_ref),
+        ))
+    ]
+    for load in loads:
+        load.start()
+    total_half[...] = jnp.zeros(total_half.shape, f32)
+    experts = lax.broadcasted_iota(jnp.int32, (ep_count, token_count), 0)
+    earlier = lax.broadcasted_iota(jnp.int32, (token_count, token_count), 0)
+    later = lax.broadcasted_iota(jnp.int32, (token_count, token_count), 1)
+    before = jnp.where(earlier < later, 1.0, 0.0).astype(bf16)
+    loads[0].wait()
+    loads[1].wait()
+    named = jnp.zeros((ep_count, token_count), f32)
+    weight_of = jnp.zeros((ep_count, token_count), f32)
+    for k in range(route_ref.shape[0]):
+        chosen_here = route_ref[pl.ds(k, 1), :] == experts
+        named = named + jnp.where(chosen_here, 1.0, 0.0)
+        weight_of = weight_of + jnp.where(chosen_here, share_ref[pl.ds(k, 1), :], 0.0)
+    rank = jnp.dot(named.astype(bf16), before, preferred_element_type=f32)
+    metas[here, pl.ds(0, ep_count), :] = jnp.where(named > 0.0, rank, -1.0)
+    metas[here, pl.ds(ep_count, ep_count), :] = weight_of
+    loads[2].wait()
+    loads[3].wait()
+    pl.semaphore_wait(barrier, ep_count + 1)
 
     @pl.when(z < count - 1)
     def _():
@@ -473,50 +546,78 @@
         def _():
             chain(kind, zi, 1).start()
 
-    def gather(i):
+    def is_early(i):
+        return (i >= far_step) & ((order(i) - z) * (order(i) - z) == 1)
+
+    def relay(kind):
+        def one(i, carry):
+            @pl.when(is_early(i))
+            def _():
+                if kind == 0:
+                    take(2, order(i))
+                take(kind, order(i))
+
+            return carry
+
+        lax.fori_loop(far_step, count, one, 0)
+
+    def picks(kind, i):
         zi = order(i)
         source = 2 * zi + x
 
+        @pl.when((i >= 1) & jnp.logical_not(is_early(i)))
+        def _():
+            if kind == 0:
+                take(2, zi)
+            take(kind, zi)
+
+        if kind == 0:
+            cross_meta(zi).start()
+        picked = jnp.dot(pick(source, other), line[kind, zi], preferred_element_type=f32)
+        pick_send[kind, zi] = picked.astype(bf16)
+        cross(kind, zi).start()
+
         @pl.when(i >= 1)
         def _():
-            take(2, zi)
-
-        cross_meta(zi).start()
-        for kind in range(2):
+            own = jnp.dot(pick(source, here), line[kind, zi], preferred_element_type=f32)
+            rows[kind, source, :, columns(part)] = own.astype(bf16)
+            far(kind, source).start()
+            near(kind, source).start()
+
+    def local_picks():
+        loads[4].wait()
+        loads[5].wait()
+        extra = jnp.dot(
+            pick(here, other), grd_ref[:, columns(across)], preferred_element_type=f32
+        )
+        pick_extra[...] = extra.astype(bf16)
+        cross_extra().start()
+        for kind, whole in enumerate((tok_ref, grd_ref)):
+            for q in range(model_width // width):
+                at = pl.ds(q * width, width)
+                own = jnp.dot(pick(here, here), whole[:, at], preferred_element_type=f32)
+                rows[kind, here, :, at] = own.astype(bf16)
+
+    def arrive(kind, i):
+        source = 2 * order(i) + 1 - x
+        cross(kind, order(i)).wait_recv()
+        if kind == 0:
+            far(kind, source).start()
+        else:
             @pl.when(i >= 1)
             def _():
-                take(kind, zi)
-
-            picked = jnp.dot(
-                pick(source, other), line[kind, zi], preferred_element_type=f32
-            )
-            pick_send[kind, zi] = picked.astype(bf16)
-            cross(kind, zi).start()
-
-            @pl.when(i >= 1)
-            def _():
-                own = jnp.dot(pick(source, here), line[kind, zi], preferred_element_type=f32)
-                rows[kind, source, :, columns(part)] = own.astype(bf16)
                 far(kind, source).start()
-                near(kind, source).start()
-
-            @pl.when(i == 0)
-            def _():
-                whole = grd_ref if kind else tok_ref
-                for q in range(model_width // width):
-                    at = pl.ds(q * width, width)
-                    own = jnp.dot(
-                        pick(source, here), whole[:, at], preferred_element_type=f32
-                    )
-                    rows[kind, source, :, at] = own.astype(bf16)
-
-    def arrive(i):
-        zi = order(i)
-        for kind in range(2):
-            cross(kind, zi).wait_recv()
-            far(kind, 2 * zi + 1 - x).start()
-            near(kind, 2 * zi + 1 - x).start()
-        cross_meta(zi).wait_recv()
+
+        near(kind, source).start()
+
+        if kind == 1:
+            cross_meta(order(i)).wait_recv()
+
+    def hand_on_first():
+        far(0, other).wait_recv()
+        onward(0, other).start()
+        cross_extra().wait_recv()
+        onward(1, other).start()
 
     def hand_on(source):
         for kind in range(2):
@@ -570,74 +671,154 @@
             if not own:
                 pair(source).start()
 
-    def pair_sum(source):
+    def pair_sum(source, zi, own):
         pair(source).wait_recv()
-        added = mine[source].astype(f32) + near_buf[source].astype(f32)
-        return added.astype(bf16)
+
+        def act(small):
+            if small:
+                at = columns(1 - plane)
+                added = mine[source, :, at].astype(f32) + near_buf[source, :, at].astype(f32)
+                half_send[source] = added.astype(bf16)
+                half_over(source).start()
+                return
+            added = (mine[source].astype(f32) + near_buf[source].astype(f32)).astype(bf16)
+            if own:
+                own_sum[zi] = added
+            else:
+                back_send[zi] = added
+                cross_back(zi, False).start()
+
+        either(zi, act)
+
+    def half_sum(source, zi, own):
+        @pl.when(is_far(zi))
+        def _():
+            half_over(source).wait_recv()
+            at = columns(plane)
+            added = mine[source, :, at].astype(f32) + near_buf[source, :, at].astype(f32)
+            added = (added + half_buf[source].astype(f32)).astype(bf16)
+            if own:
+                own_sum[zi, :, pl.ds(0, width)] = added
+            else:
+                back_send[zi, :, pl.ds(0, width)] = added
+                cross_back(zi, True).start()
 
     def merge(i):
         zi = order(i)
         source = 2 * zi + x
-        cross_back(zi).wait_recv()
         tn = (((0,), (0,)), ((), ()))
-        own_pick, other_pick = pick(source, here), pick(source, other)
-        for half in range(2):
-            at = pl.ds(half * width, width)
-            added = lax.dot_general(
-                own_pick, own_sum[zi, :, at], tn, preferred_element_type=f32
-            ) + lax.dot_general(
-                other_pick, back_buf[zi, :, at], tn, preferred_element_type=f32
-            )
-
-            @pl.when(i == 0)
-            def _():
-                total[:, at] = added
+
+        def act(small):
+            cross_back(zi, small).wait_recv()
+            for half in range(1 if small else 2):
+                at = pl.ds(half * width, width)
+                added = lax.dot_general(
+                    pick(source, here), own_sum[zi, :, at], tn, preferred_element_type=f32
+                ) + lax.dot_general(
+                    pick(source, other), back_buf[zi, :, at], tn, preferred_element_type=f32
+                )
+                if small:
+                    z_send[zi, :, at] = added.astype(bf16)
+                else:
+                    @pl.when(i == 0)
+                    def _():
+                        total[:, at] = added
+
+                    @pl.when(i >= 1)
+                    def _():
+                        z_send[zi, :, at] = added.astype(bf16)
 
             @pl.when(i >= 1)
             def _():
-                z_send[zi, :, at] = added.astype(bf16)
-
-        @pl.when(i >= 1)
-        def _():
-            line_back(zi).start()
+                line_back(zi, small).start()
+
+        either(zi, act)
+
+    def own_at(i):
+        return 2 * order(i) + x
+
+    def other_at(i):
+        return 2 * order(i) + 1 - x
+
+    last = count + 1
 
     def body(i, carry):
+        @pl.when(i == count - 1)
+        def _():
+            pair_sum(other_at(0), order(0), False)
+
+        @pl.when((i >= 1) & (i <= count))
+        def _():
+            arrive(0, i - 1)
+
+        @pl.when(i == 2)
+        def _():
+            hand_on_first()
+
+        @pl.when(i >= 3)
+        def _():
+            hand_on(other_at(i - 2))
+
+        @pl.when(i >= 2)
+        def _():
+            compute(other_at(i - 2), 0)
+
         @pl.when(i < count)
         def _():
-            gather(i)
+            picks(0, i)
+
+        @pl.when(i == 1)
+        def _():
+            relay(0)
+
+        @pl.when((i >= 1) & (i <= count))
+        def _():
+            arrive(1, i - 1)
 
         @pl.when((i >= 2) & (i <= count))
         def _():
-            hand_on(2 * order(i - 1) + x)
-
-        @pl.when(i >= 2)
-        def _():
-            compute(2 * order(i - 2) + 1 - x, 0)
-            own_sum[order(i - 2)] = pair_sum(2 * order(i - 2) + x)
+            hand_on(own_at(i - 1))
 
         @pl.when(i < count)
         def _():
-            arrive(i)
-
-        @pl.when((i >= 1) & (i <= count))
-        def _():
-            hand_on(2 * order(i - 1) + 1 - x)
-            compute(2 * order(i - 1) + x, (count - i + 1) // count)
-
-        @pl.when(i >= 2)
-        def _():
-            zi = order(i - 2)
-            back_send[zi] = pair_sum(2 * zi + 1 - x)
-            cross_back(zi).start()
-
-        @pl.when(i >= 3)
-        def _():
-            merge(i - 3)
-
-        return carry
-
-    lax.fori_loop(0, count + 2, body, 0)
-    small_near.start()
+            picks(1, i)
+
+        @pl.when(i == 1)
+        def _():
+            relay(1)
+
+        @pl.when(i == 0)
+        def _():
+            local_picks()
+            for load in loads[6:]:
+                load.wait()
+
+        @pl.when((i == 0) | ((i >= 2) & (i <= count)))
+        def _():
+            step = i - (i + count - 1) // count
+            compute(own_at(step), 1 - (step + count - 1) // count)
+
+        @pl.when(i == last)
+        def _():
+            small_near.start()
+            merge(0)
+            merge(1)
+            half_sum(other_at(count - 2), order(count - 2), False)
+            lax.fori_loop(0, chunks // 4, weights, 0)
+
+        @pl.when(i == 1)
+        def _():
+            pair_sum(own_at(0), order(0), True)
+
+        @pl.when((i >= 2) & (i <= count))
+        def _():
+            @pl.when(i >= 3)
+            def _():
+                pair_sum(other_at(i - 2), order(i - 2), False)
+
+            pair_sum(own_at(i - 1), order(i - 1), True)
+
+        return carry
 
     def weights(n, carry):
         chunk = 256
@@ -659,10 +840,16 @@
         return carry
 
     chunks = model_width // 256
+    lax.fori_loop(0, last + 1, body, 0)
+    pair_sum(other_at(count - 1), order(count - 1), False)
+    half_sum(own_at(count - 2), order(count - 2), True)
+    half_sum(own_at(count - 1), order(count - 1), True)
+    merge(count - 2)
     small_near.wait_recv()
     found_sum[...] = found_loc[...] + found_near[...]
     small_far.start()
-    lax.fori_loop(0, chunks // 2, weights, 0)
+    lax.fori_loop(chunks // 4, chunks // 2, weights, 0)
+    half_sum(other_at(count - 1), order(count - 1), False)
     small_far.wait_recv()
     found_send[...] = found_sum[...] + found_far[...]
     found_out[here] = found_send[here]
@@ -672,20 +859,37 @@
         return carry
 
     lax.fori_loop(1, ep_count, share, 0)
+    lax.fori_loop(chunks // 2, chunks, weights, 0)
     merge(count - 1)
-    lax.fori_loop(chunks // 2, chunks, weights, 0)
 
     def add(i, carry):
         zi = order(i)
-        line_got(zi).wait_recv()
-        total[...] = total[...] + z_buf[zi].astype(f32)
+
+        @pl.when(jnp.logical_not(is_far(zi)))
+        def _():
+            line_got(zi, False).wait_recv()
+            total[...] = total[...] + z_buf[zi].astype(f32)
+
+        return carry
+
+    def add_far(i, carry):
+        zi = order(i)
+
+        @pl.when(is_far(zi))
+        def _():
+            line_got(zi, True).wait_recv()
+            total_half[...] = total_half[...] + z_buf[zi, :, pl.ds(0, width)].astype(f32)
+
         return carry
 
     lax.fori_loop(1, count, add, 0)
     y_send[...] = total[:, columns(1 - plane)].astype(bf16)
     last_y.start()
+    lax.fori_loop(1, count, add_far, 0)
     last_y.wait_recv()
-    token_out[...] = (total[:, columns(plane)] + y_buf[...].astype(f32)).astype(bf16)
+    token_out[...] = (
+        total[:, columns(plane)] + total_half[...] + y_buf[...].astype(f32)
+    ).astype(bf16)
 
     def finish(zi, carry):
         for kind in range(3):
@@ -698,13 +902,13 @@
                 chain(kind, zi, 1).wait_send()
 
         cross_meta(zi).wait_send()
-        cross_back(zi).wait_send()
+        either(zi, lambda small: cross_back(zi, small).wait_send())
         for kind in range(2):
             cross(kind, zi).wait_send()
 
         @pl.when((zi < z) | (zi > z))
         def _():
-            line_back(zi).wait_send()
+            either(zi, lambda small: line_back(zi, small).wait_send())
 
         return carry
 
@@ -713,12 +917,23 @@
     def finish_source(source, carry):
         pair(source).wait_send()
 
+        @pl.when(is_far(source // 2))
+        def _():
+            half_over(source).wait_send()
+
         @pl.when((source < here) | (source > here))
         def _():
             for kind in range(2):
                 near(kind, source).wait_send()
-                far(kind, source).wait_send()
                 onward(kind, source).wait_send()
+
+        @pl.when((source < here) | (source > here))
+        def _():
+            far(0, source).wait_send()
+
+        @pl.when((source // 2 < z) | (source // 2 > z))
+        def _():
+            far(1, source).wait_send()
 
         return carry
 
@@ -729,12 +944,13 @@
         return carry
 
     lax.fori_loop(1, ep_count, finish_found, 0)
+    cross_extra().wait_send()
     last_y.wait_send()
     small_near.wait_send()
     small_far.wait_send()
 
 
-def fused(tokens, grads, meta, w_gate, w_up, w_down, capacity, width):
+def fused(tokens, grads, routes, shares, w_gate, w_up, w_down, capacity, width):
     f32, bf16 = jnp.float32, jnp.bfloat16
     ep_count = lax.axis_size("ep")
     count = ep_count // 2
@@ -745,9 +961,17 @@
     small = vm((ep_count, 1, token_count), f32)
     half = (capacity, 2 * width)
     scratch = [
+        vm(tokens.shape, bf16),
+        vm(tokens.shape, bf16),
+        vm(routes.shape, jnp.int32),
+        vm(routes.shape, f32),
+        vm(w_gate.shape, bf16),
+        vm(w_up.shape, bf16),
+        vm(w_down.shape, bf16),
         vm((2, count, token_count, width), bf16),
-        vm((ep_count,) + meta.shape, f32),
+        vm((ep_count, 2 * ep_count, token_count), f32),
         vm((2, count, capacity, width), bf16),
+        vm((capacity, width), bf16),
         vm((2, ep_count, capacity, model_width), bf16),
         vm((ep_count, capacity, units), bf16),
         vm((ep_count, capacity, units), bf16),
@@ -758,23 +982,28 @@
         vm((count,) + half, bf16),
         vm((count,) + half, bf16),
         vm((count,) + half, bf16),
+        vm((ep_count, capacity, width), bf16),
+        vm((ep_count, capacity, width), bf16),
         vm((count, token_count, 2 * width), bf16),
         vm((count, token_count, 2 * width), bf16),
         vm((token_count, 2 * width), f32),
+        vm((token_count, width), f32),
         vm((token_count, width), bf16),
         vm((token_count, width), bf16),
         small, small, small, small, small,
         dma((2, 3, count)), dma((3, count)),
         dma((count,)), dma((count,)),
         dma((2, count)), dma((2, count)),
+        dma((1,)), dma((1,)),
         dma((2, ep_count)), dma((2, ep_count)),
         dma((2, ep_count)), dma((2, ep_count)),
         dma((2, ep_count)), dma((2, ep_count)),
         dma((ep_count,)), dma((ep_count,)),
+        dma((ep_count,)), dma((ep_count,)),
         dma((count,)), dma((count,)),
         dma((count,)), dma((count,)),
         dma((1,)), dma((1,)), dma((2,)), dma((2,)),
-        dma((ep_count,)), dma((ep_count,)),
+        dma((ep_count,)), dma((ep_count,)), dma((9,)),
     ]
     return pl.pallas_call(
         fused_kernel,
@@ -785,40 +1014,71 @@
             jax.ShapeDtypeStruct((model_width, units), f32),
             jax.ShapeDtypeStruct((units, model_width), f32),
         ),
-        in_specs=[pl.BlockSpec(memory_space=pltpu.VMEM)] * 6,
+        in_specs=[pl.BlockSpec(memory_space=pltpu.HBM)] * 7,
         out_specs=(pl.BlockSpec(memory_space=pltpu.VMEM),) * 5,
         scratch_shapes=scratch,
         compiler_params=pltpu.CompilerParams(
-            collective_id=2, has_side_effects=True, vmem_limit_bytes=60 * 1024 * 1024
+            collective_id=2, has_side_effects=True, vmem_limit_bytes=46 * 1024 * 1024
         ),
-    )(tokens, grads, meta, w_gate, w_up, w_down)
+    )(tokens, grads, routes, shares, w_gate, w_up, w_down)
+
+
+def store_kernel(
+    token_ref, found_ref, gate_ref, up_ref, down_ref, route_ref,
+    token_out, found_out, gate_out, up_out, down_out, found_buf, sems,
+):
+    copies = [
+        pltpu.make_async_copy(src, dst, sems.at[n])
+        for n, (src, dst) in enumerate((
+            (gate_ref, gate_out), (up_ref, up_out), (down_ref, down_out), (token_ref, token_out),
+        ))
+    ]
+    for copy in copies:
+        copy.start()
+    for k in range(route_ref.shape[0]):
+        row = jnp.zeros((1, route_ref.shape[1]), jnp.float32)
+        for expert in range(found_ref.shape[0]):
+            hit = route_ref[pl.ds(k, 1), :] == expert
+            row = row + jnp.where(hit, found_ref[expert], 0.0)
+        found_buf[pl.ds(k, 1), :] = row
+    last = pltpu.make_async_copy(found_buf, found_out, sems.at[4])
+    last.start()
+    for copy in copies:
+        copy.wait()
+    last.wait()
+
+
+def store(token_grad, found, gate_grads, up_grads, down_grads, routes):
+    arrays = (token_grad, found, gate_grads, up_grads, down_grads)
+    outs = [jax.ShapeDtypeStruct(a.shape, a.dtype) for a in arrays]
+    outs[1] = jax.ShapeDtypeStruct(routes.shape, jnp.float32)
+    return pl.pallas_call(
+        store_kernel,
+        out_shape=tuple(outs),
+        in_specs=[pl.BlockSpec(memory_space=pltpu.VMEM)] * 6,
+        out_specs=(pl.BlockSpec(memory_space=pltpu.HBM),) * 5,
+        scratch_shapes=[pltpu.VMEM(routes.shape, jnp.float32), pltpu.SemaphoreType.DMA((5,))],
+        compiler_params=pltpu.CompilerParams(vmem_limit_bytes=8 * 1024 * 1024),
+    )(*arrays, routes)
 
 
 def gathered(tokens, routes, gate_weights, out_grad, w_gate, w_up, w_down):
-    f32, bf16 = jnp.float32, jnp.bfloat16
     ep_count = lax.axis_size("ep")
     token_count, model_width = tokens.shape
     capacity = token_count * routes.shape[1] * 5 // (4 * ep_count)
     width = model_width // lax.axis_size("tp")
-    by_expert = routes.T
-    match = by_expert[None, :, :] == jnp.arange(ep_count, dtype=jnp.int32)[:, None, None]
-    named = jnp.any(match, axis=1)
-    before = jnp.arange(token_count)[:, None] < jnp.arange(token_count)[None, :]
-    rank = jnp.dot(named.astype(bf16), before.astype(bf16), preferred_element_type=f32)
-    rank = jnp.where(named, rank, -1.0)
-    weight_of = jnp.sum(jnp.where(match, gate_weights.T[None, :, :], 0.0), axis=1)
-    meta = jnp.concatenate([rank, weight_of], axis=0)
-    token_grad, found, gate_grads, up_grads, down_grads = fused(
-        tokens, out_grad, meta, w_gate[0], w_up[0], w_down[0], capacity, width
-    )
-    gate_grad = jnp.sum(jnp.where(match, found, 0.0), axis=0).T
-    return (token_grad, gate_grad, gate_grads[None], up_grads[None], down_grads[None])
+    arrays = (tokens, out_grad, routes.T, gate_weights.T, w_gate[0], w_up[0], w_down[0])
+    arrays = [pltpu.with_memory_space_constraint(array, pltpu.HBM) for array in arrays]
+    parts = fused(*arrays, capacity, width)
+    token_grad, gate_grad, gate_grads, up_grads, down_grads = store(*parts, routes.T)
+    return (token_grad, gate_grad.T, gate_grads[None], up_grads[None], down_grads[None])
 
 
 def chosen(*args):
     tokens, w_gate = args[0], args[4]
-    block_bytes = lax.axis_size("ep") * tokens.size * 2
-    if block_bytes <= 16 * 1024 * 1024 and w_gate.shape[0] == 1:
+    ep_count = lax.axis_size("ep")
+    block_bytes = ep_count * tokens.size * 2
+    if block_bytes <= 16 * 1024 * 1024 and w_gate.shape[0] == 1 and ep_count == 8:
         return gathered(*args)
     return local(*args)
 

time: 142 us -> 103 us (0.73)
  the two profiles are of different devices: /device:TPU:0 before, /device:TPU:9 now
where the time goes in v2:
time: 103 us
  Pallas kernels  102 us (99%)
    pallas_call x1, Pallas kernels, fused(): pl.pallas_call(fused_kernel, out_shape=(jax.ShapeDtypeStruct((token_count...  99.7 us
    pallas_call x1, Pallas kernels, store(): pl.pallas_call(store_kernel, out_shape=tuple(outs), in_specs=[pl.BlockSpe...  2.76 us

profile of v2, /device:TPU:9, one launch (start us, length us, event | category | flops | bytes accessed | tf_op | source)
XLA Modules:
  0.0 103.2 jit_solution(1818816690467786079)
XLA Ops:
  0.6 0.0 copy-start
  0.6 99.7 %shard_map.110 = (bf16[256,512]{1,0:T(8,128)(2,1)S(1)}, f32[8,1,256]{2,1,0:T(1,128)S(1)}, f32[2048,256]{1,0:T(8,128)S(1)}, f32[2048,256]{1,0:T(8,128)S(1)}, f32[256,2048]{1,0:T(8,128)S(1)}) custom-call(bf16[256,2048]{1,0:T(8,128)(2,1)} %tok_hbm.1, bf16[256,2048]{1,0:T(8,128)(2,1)} %grd_hbm.1, s32[4,256]{1,0:T(4,128)} %bitcast.9, f32[4,256]{1,0:T(4,128)} %bitcast.14, ...), custom_call_target="tpu_custom_call" | custom-call | tf_op jit(solution)/shard_map/pallas_call | solution.py:1008
  100.4 0.0 copy-done
  100.4 2.8 %shard_map.111 = (bf16[256,512]{1,0:T(8,128)(2,1)}, f32[4,256]{1,0:T(4,128)}, f32[2048,256]{1,0:T(8,128)}, f32[2048,256]{1,0:T(8,128)}, f32[256,2048]{1,0:T(8,128)}) custom-call(bf16[256,512]{1,0:T(8,128)(2,1)S(1)} %get-tuple-element.15.token_ref, f32[8,1,256]{2,1,0:T(1,128)S(1)} %get-tuple-element.16.found_ref, f32[2048,256]{1,0:T(8,128)S(1)} %get-tuple-element.17.gate_ref, ...), custom_call_target="tpu_custom_call" | custom-call | tf_op jit(solution)/shard_map/pallas_call | solution.py:1055
Async XLA Ops:
  0.6 99.8 %copy-start = (s32[256,4]{0,1:T(4,128)S(1)}, s32[256,4]{0,1:T(4,128)}, u32[]{:S(2)}) copy-start(s32[256,4]{0,1:T(4,128)} %param.8) | copy-start | bytes 12292

commit v3 on v2

--- a/solution.py
+++ b/solution.py
@@ -360,11 +360,11 @@
 def fused_kernel(
     tok_hbm, grd_hbm, route_hbm, share_hbm, gate_hbm, up_hbm, down_hbm,
     token_out, found_out, gate_out, up_out, down_out,
-    tok_ref, grd_ref, route_ref, share_ref, gate_ref, up_ref, down_ref, line, metas, pick_send, pick_extra, rows, gate_g, up_g, hid,
+    tok_ref, grd_ref, route_ref, share_ref, gate_ref, up_ref, down_ref, line, line_extra, metas, pick_send, rows, gate_g, up_g, hid,
     near_send, near_buf, mine, own_sum, back_send, back_buf,
     half_send, half_buf, z_send, z_buf, total, total_half, y_send, y_buf,
     found_loc, found_near, found_sum, found_far, found_send,
-    chain_s, chain_r, xm_s, xm_r, x_s, x_r, e_s, e_r, n_s, n_r, f_s, f_r, o_s, o_r,
+    chain_s, chain_r, xm_s, xm_r, x_s, x_r, u_s, u_r, n_s, n_r, f_s, f_r, o_s, o_r,
     c_s, c_r, h_s, h_r, b_s, b_r, z_s, z_r, y_s, y_r, sm_s, sm_r, l_s, l_r, in_s,
 ):
     f32, bf16 = jnp.float32, jnp.bfloat16
@@ -388,11 +388,24 @@
             bit = 2 * bit
         return mixed
 
+    inward = (2 * z) // count
+    middle = (2 * z * (count - 1 - z) + count * count - 1) // (count * count)
+
+    def place(i):
+        return order(i + middle * (i // far_step) * (1 - 2 * (i % 2)))
+
     def chain(kind, zi, way):
         ref = metas.at[2 * zi + x] if kind == 2 else line.at[kind, zi]
         to = here + 2 - 4 * way
         return remote(ref, ref, chain_s.at[way, kind, zi], chain_r.at[kind, zi], (to, part))
 
+    def chain_extra(kind, way):
+        whole = grd_ref if kind else tok_ref
+        return remote(
+            whole.at[:, columns(across)], line_extra.at[way, kind],
+            u_s.at[way, kind], u_r.at[way, kind], (here + 2 - 4 * way, part),
+        )
+
     def cross_meta(zi):
         ref = metas.at[2 * zi + x]
         return remote(ref, ref, xm_s.at[zi], xm_r.at[zi], (other, part))
@@ -403,12 +416,6 @@
             x_s.at[kind, zi], x_r.at[kind, zi], (other, part),
         )
 
-    def cross_extra():
-        return remote(
-            pick_extra, rows.at[1, here, :, columns(across)],
-            e_s.at[0], e_r.at[0], (other, part),
-        )
-
     def forward(kind, source, owner, sent, got, to):
         ref = rows.at[kind, source, :, columns(owner)]
         return remote(ref, ref, sent.at[kind, source], got.at[kind, source], (here, to))
@@ -446,16 +453,18 @@
             b_s.at[zi], b_r.at[zi], (other, part),
         )
 
-    def line_back(zi, small):
+    def line_back(zi, small, half=0):
+        at = pl.ds(0, width) if small else columns(half)
         return remote(
-            cut(z_send, zi, small), cut(z_buf, z, small),
-            z_s.at[zi], z_r.at[z], (2 * zi + x, part),
-        )
-
-    def line_got(zi, small):
+            z_send.at[zi, :, at], z_buf.at[z, :, at],
+            z_s.at[half, zi], z_r.at[half, z], (2 * zi + x, part),
+        )
+
+    def line_got(zi, small, half=0):
+        at = pl.ds(0, width) if small else columns(half)
         return remote(
-            cut(z_send, zi, small), cut(z_buf, zi, small),
-            z_s.at[zi], z_r.at[zi], (2 * zi + x, part),
+            z_send.at[zi, :, at], z_buf.at[zi, :, at],
+            z_s.at[half, zi], z_r.at[half, zi], (2 * zi + x, part),
         )
 
     def either(zi, act):
@@ -487,12 +496,16 @@
     pl.semaphore_signal(barrier, inc=1, device_id=(here, beside), device_id_type=MESH)
     pl.semaphore_signal(barrier, inc=1, device_id=(here, across), device_id_type=MESH)
 
-    def hail(j, carry):
-        peer = (here + j) % ep_count
-        pl.semaphore_signal(barrier, inc=1, device_id=(peer, part), device_id_type=MESH)
-        return carry
-
-    lax.fori_loop(1, ep_count, hail, 0)
+    pl.semaphore_signal(barrier, inc=1, device_id=(other, part), device_id_type=MESH)
+
+    @pl.when(z > 0)
+    def _():
+        pl.semaphore_signal(barrier, inc=1, device_id=(here - 2, part), device_id_type=MESH)
+
+    @pl.when(z < count - 1)
+    def _():
+        pl.semaphore_signal(barrier, inc=1, device_id=(here + 2, part), device_id_type=MESH)
+
     loads = [
         pltpu.make_async_copy(src, dst, in_s.at[n])
         for n, (src, dst) in enumerate((
@@ -523,7 +536,7 @@
     metas[here, pl.ds(ep_count, ep_count), :] = weight_of
     loads[2].wait()
     loads[3].wait()
-    pl.semaphore_wait(barrier, ep_count + 1)
+    pl.semaphore_wait(barrier, 4 + middle)
 
     @pl.when(z < count - 1)
     def _():
@@ -546,26 +559,37 @@
         def _():
             chain(kind, zi, 1).start()
 
-    def is_early(i):
-        return (i >= far_step) & ((order(i) - z) * (order(i) - z) == 1)
-
-    def relay(kind):
-        def one(i, carry):
-            @pl.when(is_early(i))
-            def _():
-                if kind == 0:
-                    take(2, order(i))
-                take(kind, order(i))
-
-            return carry
-
-        lax.fori_loop(far_step, count, one, 0)
+    def is_next(zi):
+        return (zi - z) * (zi - z) == 1
+
+    def send_extra(way):
+        chain_extra(0, way).start()
+        chain_extra(1, way).start()
+
+    def hand_on_extra(i):
+        zi = place(i)
+        source = 2 * zi + x
+        way = (zi - z + 1) // 2
+        for kind in range(2):
+            chain_extra(kind, way).wait_recv()
+            own = jnp.dot(
+                pick(source, here), line_extra[way, kind], preferred_element_type=f32
+            )
+            rows[kind, source, :, columns(across)] = own.astype(bf16)
+            onward(kind, source).start()
+
+    def relay(kind, i):
+        @pl.when(middle == 1)
+        def _():
+            if kind == 0:
+                take(2, place(i))
+            take(kind, place(i))
 
     def picks(kind, i):
-        zi = order(i)
+        zi = place(i)
         source = 2 * zi + x
 
-        @pl.when((i >= 1) & jnp.logical_not(is_early(i)))
+        @pl.when((i == 1) | ((i > 1) & (middle == 0)))
         def _():
             if kind == 0:
                 take(2, zi)
@@ -581,17 +605,16 @@
         def _():
             own = jnp.dot(pick(source, here), line[kind, zi], preferred_element_type=f32)
             rows[kind, source, :, columns(part)] = own.astype(bf16)
-            far(kind, source).start()
+
+            @pl.when(jnp.logical_not(is_next(zi)))
+            def _():
+                far(kind, source).start()
+
             near(kind, source).start()
 
     def local_picks():
         loads[4].wait()
         loads[5].wait()
-        extra = jnp.dot(
-            pick(here, other), grd_ref[:, columns(across)], preferred_element_type=f32
-        )
-        pick_extra[...] = extra.astype(bf16)
-        cross_extra().start()
         for kind, whole in enumerate((tok_ref, grd_ref)):
             for q in range(model_width // width):
                 at = pl.ds(q * width, width)
@@ -599,25 +622,12 @@
                 rows[kind, here, :, at] = own.astype(bf16)
 
     def arrive(kind, i):
-        source = 2 * order(i) + 1 - x
-        cross(kind, order(i)).wait_recv()
-        if kind == 0:
-            far(kind, source).start()
-        else:
-            @pl.when(i >= 1)
-            def _():
-                far(kind, source).start()
-
+        source = 2 * place(i) + 1 - x
+        cross(kind, place(i)).wait_recv()
+        far(kind, source).start()
         near(kind, source).start()
-
         if kind == 1:
-            cross_meta(order(i)).wait_recv()
-
-    def hand_on_first():
-        far(0, other).wait_recv()
-        onward(0, other).start()
-        cross_extra().wait_recv()
-        onward(1, other).start()
+            cross_meta(place(i)).wait_recv()
 
     def hand_on(source):
         for kind in range(2):
@@ -704,7 +714,7 @@
                 cross_back(zi, True).start()
 
     def merge(i):
-        zi = order(i)
+        zi = place(i)
         source = 2 * zi + x
         tn = (((0,), (0,)), ((), ()))
 
@@ -728,96 +738,123 @@
                     def _():
                         z_send[zi, :, at] = added.astype(bf16)
 
-            @pl.when(i >= 1)
+            if small:
+                line_back(zi, True).start()
+            else:
+                @pl.when(i >= 1)
+                def _():
+                    line_back(zi, False, 1 - plane).start()
+                    line_back(zi, False, plane).start()
+
+        either(zi, act)
+
+    def own_at(i):
+        return 2 * place(i) + x
+
+    def other_at(i):
+        return 2 * place(i) + 1 - x
+
+    last = count - 1
+
+    def body(i, carry):
+        @pl.when(i == last)
+        def _():
+            pair_sum(other_at(0), place(0), False)
+
+        @pl.when(i >= 1)
+        def _():
+            arrive(0, i - 1)
+
+        @pl.when(i >= 2)
+        def _():
+            hand_on(other_at(i - 2))
+            compute(other_at(i - 2), 0)
+
+        @pl.when(i < count)
+        def _():
+            picks(0, i)
+
+        @pl.when((i == 1) | (i == 2))
+        def _():
+            relay(0, i + 1)
+
+        @pl.when(i >= 1)
+        def _():
+            arrive(1, i - 1)
+
+        @pl.when(i == count)
+        def _():
+            pair_sum(own_at(last - 1), place(last - 1), True)
+            pair_sum(other_at(last - 1), place(last - 1), False)
+
+        @pl.when(i < count)
+        def _():
+            picks(1, i)
+
+        @pl.when((i == 1) | (i == 2))
+        def _():
+            relay(1, i + 1)
+
+        @pl.when(i == 0)
+        def _():
+            local_picks()
+
+            @pl.when(middle == 0)
             def _():
-                line_back(zi, small).start()
-
-        either(zi, act)
-
-    def own_at(i):
-        return 2 * order(i) + x
-
-    def other_at(i):
-        return 2 * order(i) + 1 - x
-
-    last = count + 1
-
-    def body(i, carry):
-        @pl.when(i == count - 1)
-        def _():
-            pair_sum(other_at(0), order(0), False)
-
-        @pl.when((i >= 1) & (i <= count))
-        def _():
-            arrive(0, i - 1)
-
-        @pl.when(i == 2)
-        def _():
-            hand_on_first()
-
-        @pl.when(i >= 3)
-        def _():
-            hand_on(other_at(i - 2))
-
-        @pl.when(i >= 2)
-        def _():
-            compute(other_at(i - 2), 0)
-
-        @pl.when(i < count)
-        def _():
-            picks(0, i)
-
-        @pl.when(i == 1)
-        def _():
-            relay(0)
-
-        @pl.when((i >= 1) & (i <= count))
-        def _():
-            arrive(1, i - 1)
-
-        @pl.when((i >= 2) & (i <= count))
-        def _():
-            hand_on(own_at(i - 1))
-
-        @pl.when(i < count)
-        def _():
-            picks(1, i)
-
-        @pl.when(i == 1)
-        def _():
-            relay(1)
-
-        @pl.when(i == 0)
-        def _():
-            local_picks()
+                send_extra(inward)
+
             for load in loads[6:]:
                 load.wait()
 
-        @pl.when((i == 0) | ((i >= 2) & (i <= count)))
+        @pl.when((i == 1) & (middle == 1))
+        def _():
+            send_extra(inward)
+
+        @pl.when((i == 2) & (middle == 1))
+        def _():
+            send_extra(1 - inward)
+
+        @pl.when(i >= 3)
+        def _():
+            @pl.when(is_next(place(i - 1)))
+            def _():
+                hand_on_extra(i - 1)
+
+            @pl.when(jnp.logical_not(is_next(place(i - 1))))
+            def _():
+                hand_on(own_at(i - 1))
+
+        @pl.when(i == count)
+        def _():
+            hand_on_extra(1)
+
+        @pl.when((i == 0) | (i >= 3))
         def _():
             step = i - (i + count - 1) // count
             compute(own_at(step), 1 - (step + count - 1) // count)
 
+        @pl.when(i == count)
+        def _():
+            pair_sum(own_at(last), place(last), True)
+
+        @pl.when(i == 1)
+        def _():
+            pair_sum(own_at(0), place(0), True)
+
         @pl.when(i == last)
         def _():
-            small_near.start()
-            merge(0)
-            merge(1)
-            half_sum(other_at(count - 2), order(count - 2), False)
-            lax.fori_loop(0, chunks // 4, weights, 0)
-
-        @pl.when(i == 1)
-        def _():
-            pair_sum(own_at(0), order(0), True)
-
-        @pl.when((i >= 2) & (i <= count))
-        def _():
-            @pl.when(i >= 3)
-            def _():
-                pair_sum(other_at(i - 2), order(i - 2), False)
-
-            pair_sum(own_at(i - 1), order(i - 1), True)
-
+            pair_sum(other_at(1), place(1), False)
+
+        return carry
+
+    def closing(j, carry):
+        is_other = middle + j - 2 * middle * j
+
+        @pl.when(is_other == 1)
+        def _():
+            hand_on(other_at(last))
+
+        compute(own_at(1) + (other_at(last) - own_at(1)) * is_other, 0)
         return carry
 
     def weights(n, carry):
@@ -840,16 +877,22 @@
         return carry
 
     chunks = model_width // 256
-    lax.fori_loop(0, last + 1, body, 0)
-    pair_sum(other_at(count - 1), order(count - 1), False)
-    half_sum(own_at(count - 2), order(count - 2), True)
-    half_sum(own_at(count - 1), order(count - 1), True)
-    merge(count - 2)
+    lax.fori_loop(0, count + 1, body, 0)
+    lax.fori_loop(0, 2, closing, 0)
+    small_near.start()
+    pair_sum(other_at(last), place(last), False)
+    pair_sum(own_at(1), place(1), True)
+    merge(1)
+    half_sum(other_at(last - 1), place(last - 1), False)
+    half_sum(own_at(last - 1), place(last - 1), True)
+    merge(0)
     small_near.wait_recv()
     found_sum[...] = found_loc[...] + found_near[...]
     small_far.start()
-    lax.fori_loop(chunks // 4, chunks // 2, weights, 0)
-    half_sum(other_at(count - 1), order(count - 1), False)
+    lax.fori_loop(0, chunks // 4, weights, 0)
+    half_sum(own_at(last), place(last), True)
+    merge(last - 1)
+    half_sum(other_at(last), place(last), False)
     small_far.wait_recv()
     found_send[...] = found_sum[...] + found_far[...]
     found_out[here] = found_send[here]
@@ -859,18 +902,22 @@
         return carry
 
     lax.fori_loop(1, ep_count, share, 0)
-    lax.fori_loop(chunks // 2, chunks, weights, 0)
-    merge(count - 1)
-
-    def add(i, carry):
-        zi = order(i)
-
-        @pl.when(jnp.logical_not(is_far(zi)))
-        def _():
-            line_got(zi, False).wait_recv()
-            total[...] = total[...] + z_buf[zi].astype(f32)
-
-        return carry
+    lax.fori_loop(chunks // 4, chunks, weights, 0)
+    merge(last)
+
+    def add(half):
+        def one(i, carry):
+            zi = order(i)
+
+            @pl.when(jnp.logical_not(is_far(zi)))
+            def _():
+                at = columns(half)
+                line_got(zi, False, half).wait_recv()
+                total[:, at] = total[:, at] + z_buf[zi, :, at].astype(f32)
+
+            return carry
+
+        lax.fori_loop(1, count, one, 0)
 
     def add_far(i, carry):
         zi = order(i)
@@ -882,72 +929,92 @@
 
         return carry
 
-    lax.fori_loop(1, count, add, 0)
+    def finish(zi, carry):
+        for kind in range(3):
+            @pl.when((zi <= z) & (z < count - 1))
+            def _():
+                chain(kind, zi, 0).wait_send()
+
+            @pl.when((zi >= z) & (z > 0))
+            def _():
+                chain(kind, zi, 1).wait_send()
+
+        cross_meta(zi).wait_send()
+        either(zi, lambda small: cross_back(zi, small).wait_send())
+        for kind in range(2):
+            cross(kind, zi).wait_send()
+
+        return carry
+
+    def finish_source(source, carry):
+        pair(source).wait_send()
+
+        @pl.when(is_far(source // 2))
+        def _():
+            half_over(source).wait_send()
+
+        @pl.when((source < here) | (source > here))
+        def _():
+            for kind in range(2):
+                near(kind, source).wait_send()
+                onward(kind, source).wait_send()
+
+        gap = source // 2 - z
+        across_line = (source - x) % 2
+
+        @pl.when((across_line == 1) | (gap * gap > 1))
+        def _():
+            for kind in range(2):
+                far(kind, source).wait_send()
+
+        return carry
+
+    def finish_extra(way):
+        chain_extra(0, way).wait_send()
+        chain_extra(1, way).wait_send()
+
+    add(1 - plane)
     y_send[...] = total[:, columns(1 - plane)].astype(bf16)
     last_y.start()
+    lax.fori_loop(0, count, finish, 0)
+    lax.fori_loop(0, ep_count, finish_source, 0)
+    add(plane)
+    finish_extra(inward)
+
+    @pl.when(middle == 1)
+    def _():
+        finish_extra(1 - inward)
+
+    small_near.wait_send()
+    small_far.wait_send()
+
+    def finish_found(j, carry):
+        last_found(j).wait()
+        return carry
+
+    lax.fori_loop(1, ep_count, finish_found, 0)
     lax.fori_loop(1, count, add_far, 0)
     last_y.wait_recv()
     token_out[...] = (
         total[:, columns(plane)] + total_half[...] + y_buf[...].astype(f32)
     ).astype(bf16)
 
-    def finish(zi, carry):
-        for kind in range(3):
-            @pl.when((zi <= z) & (z < count - 1))
-            def _():
-                chain(kind, zi, 0).wait_send()
-
-            @pl.when((zi >= z) & (z > 0))
-            def _():
-                chain(kind, zi, 1).wait_send()
-
-        cross_meta(zi).wait_send()
-        either(zi, lambda small: cross_back(zi, small).wait_send())
-        for kind in range(2):
-            cross(kind, zi).wait_send()
-
-        @pl.when((zi < z) | (zi > z))
-        def _():
-            either(zi, lambda small: line_back(zi, small).wait_send())
-
-        return carry
-
-    lax.fori_loop(0, count, finish, 0)
-
-    def finish_source(source, carry):
-        pair(source).wait_send()
-
-        @pl.when(is_far(source // 2))
-        def _():
-            half_over(source).wait_send()
-
-        @pl.when((source < here) | (source > here))
-        def _():
-            for kind in range(2):
-                near(kind, source).wait_send()
-                onward(kind, source).wait_send()
-
-        @pl.when((source < here) | (source > here))
-        def _():
-            far(0, source).wait_send()
-
-        @pl.when((source // 2 < z) | (source // 2 > z))
-        def _():
-            far(1, source).wait_send()
-
-        return carry
-
-    lax.fori_loop(0, ep_count, finish_source, 0)
-
-    def finish_found(j, carry):
-        last_found(j).wait()
-        return carry
-
-    lax.fori_loop(1, ep_count, finish_found, 0)
-    cross_extra().wait_send()
+    def finish_line(i, carry):
+        zi = order(i)
+
+        @pl.when(is_far(zi))
+        def _():
+            line_back(zi, True).wait_send()
+
+        @pl.when(jnp.logical_not(is_far(zi)))
+        def _():
+            line_back(zi, False, 0).wait_send()
+            line_back(zi, False, 1).wait_send()
+
+        return carry
+
+    lax.fori_loop(1, count, finish_line, 0)
     last_y.wait_send()
-    small_near.wait_send()
-    small_far.wait_send()
 
 
 def fused(tokens, grads, routes, shares, w_gate, w_up, w_down, capacity, width):
@@ -969,9 +1036,9 @@
         vm(w_up.shape, bf16),
         vm(w_down.shape, bf16),
         vm((2, count, token_count, width), bf16),
+        vm((2, 2, token_count, width), bf16),
         vm((ep_count, 2 * ep_count, token_count), f32),
         vm((2, count, capacity, width), bf16),
-        vm((capacity, width), bf16),
         vm((2, ep_count, capacity, model_width), bf16),
         vm((ep_count, capacity, units), bf16),
         vm((ep_count, capacity, units), bf16),
@@ -994,14 +1061,14 @@
         dma((2, 3, count)), dma((3, count)),
         dma((count,)), dma((count,)),
         dma((2, count)), dma((2, count)),
-        dma((1,)), dma((1,)),
+        dma((2, 2)), dma((2, 2)),
         dma((2, ep_count)), dma((2, ep_count)),
         dma((2, ep_count)), dma((2, ep_count)),
         dma((2, ep_count)), dma((2, ep_count)),
         dma((ep_count,)), dma((ep_count,)),
         dma((ep_count,)), dma((ep_count,)),
         dma((count,)), dma((count,)),
-        dma((count,)), dma((count,)),
+        dma((2, count)), dma((2, count)),
         dma((1,)), dma((1,)), dma((2,)), dma((2,)),
         dma((ep_count,)), dma((ep_count,)), dma((9,)),
     ]
@@ -1018,7 +1085,7 @@
         out_specs=(pl.BlockSpec(memory_space=pltpu.VMEM),) * 5,
         scratch_shapes=scratch,
         compiler_params=pltpu.CompilerParams(
-            collective_id=2, has_side_effects=True, vmem_limit_bytes=46 * 1024 * 1024
+            collective_id=2, has_side_effects=True, vmem_limit_bytes=47 * 1024 * 1024
         ),
     )(tokens, grads, routes, shares, w_gate, w_up, w_down)
 

time: 103 us -> 99.3 us (0.964)
  the two profiles are of different devices: /device:TPU:9 before, /device:TPU:0 now
where the time goes in v3:
time: 99.3 us; the launch traced here: 99.1 us
  Pallas kernels  98.4 us (99%)
    pallas_call x1, Pallas kernels, fused(): pl.pallas_call(fused_kernel, out_shape=(jax.ShapeDtypeStruct((token_count...  95.7 us
    pallas_call x1, Pallas kernels, store(): pl.pallas_call(store_kernel, out_shape=tuple(outs), in_specs=[pl.BlockSpe...  2.76 us

profile of v3, /device:TPU:0, one launch (start us, length us, event | category | flops | bytes accessed | tf_op | source)
XLA Modules:
  0.0 99.1 jit_solution(7373810286237267428)
XLA Ops:
  0.6 0.0 copy-start
  0.6 95.7 %shard_map.110 = (bf16[256,512]{1,0:T(8,128)(2,1)S(1)}, f32[8,1,256]{2,1,0:T(1,128)S(1)}, f32[2048,256]{1,0:T(8,128)S(1)}, f32[2048,256]{1,0:T(8,128)S(1)}, f32[256,2048]{1,0:T(8,128)S(1)}) custom-call(bf16[256,2048]{1,0:T(8,128)(2,1)} %tok_hbm.1, bf16[256,2048]{1,0:T(8,128)(2,1)} %grd_hbm.1, s32[4,256]{1,0:T(4,128)} %bitcast.9, f32[4,256]{1,0:T(4,128)} %bitcast.14, ...), custom_call_target="tpu_custom_call" | custom-call | tf_op jit(solution)/shard_map/pallas_call | solution.py:1075
  96.3 0.0 copy-done
  96.3 2.8 %shard_map.111 = (bf16[256,512]{1,0:T(8,128)(2,1)}, f32[4,256]{1,0:T(4,128)}, f32[2048,256]{1,0:T(8,128)}, f32[2048,256]{1,0:T(8,128)}, f32[256,2048]{1,0:T(8,128)}) custom-call(bf16[256,512]{1,0:T(8,128)(2,1)S(1)} %get-tuple-element.15.token_ref, f32[8,1,256]{2,1,0:T(1,128)S(1)} %get-tuple-element.16.found_ref, f32[2048,256]{1,0:T(8,128)S(1)} %get-tuple-element.17.gate_ref, ...), custom_call_target="tpu_custom_call" | custom-call | tf_op jit(solution)/shard_map/pallas_call | solution.py:1122
Async XLA Ops:
  0.6 95.7 %copy-start = (s32[256,4]{0,1:T(4,128)S(1)}, s32[256,4]{0,1:T(4,128)}, u32[]{:S(2)}) copy-start(s32[256,4]{0,1:T(4,128)} %param.8) | copy-start | bytes 12292

commit v4 on v3

--- a/solution.py
+++ b/solution.py
@@ -361,11 +361,11 @@
     tok_hbm, grd_hbm, route_hbm, share_hbm, gate_hbm, up_hbm, down_hbm,
     token_out, found_out, gate_out, up_out, down_out,
     tok_ref, grd_ref, route_ref, share_ref, gate_ref, up_ref, down_ref, line, line_extra, metas, pick_send, rows, gate_g, up_g, hid,
-    near_send, near_buf, mine, own_sum, back_send, back_buf,
-    half_send, half_buf, z_send, z_buf, total, total_half, y_send, y_buf,
+    near_send, near_buf, mine, own_sum, back_send,
+    wide_buf, half_send, half_buf, narrow_send, narrow_buf, total, total_half, y_send, y_buf,
     found_loc, found_near, found_sum, found_far, found_send,
     chain_s, chain_r, xm_s, xm_r, x_s, x_r, u_s, u_r, n_s, n_r, f_s, f_r, o_s, o_r,
-    c_s, c_r, h_s, h_r, b_s, b_r, z_s, z_r, y_s, y_r, sm_s, sm_r, l_s, l_r, in_s,
+    c_s, c_r, h_s, h_r, w_s, w_r, z_s, z_r, y_s, y_r, sm_s, sm_r, l_s, l_r, in_s,
 ):
     f32, bf16 = jnp.float32, jnp.bfloat16
     ep_count, here, part, beside, across = partners()
@@ -442,29 +442,21 @@
         )
 
     def is_far(zi):
-        return order(zi) >= far_step
-
-    def cut(ref, zi, small):
-        return ref.at[zi, :, pl.ds(0, width)] if small else ref.at[zi]
-
-    def cross_back(zi, small):
+        return (zi - z) * (zi - z) >= far_step * far_step
+
+    def wide(source, own):
+        ref = own_sum.at[source // 2] if own else back_send.at[source // 2]
+        return remote(ref, wide_buf.at[here], w_s.at[source], w_r.at[here], (source, part))
+
+    def wide_got(sender):
         return remote(
-            cut(back_send, zi, small), cut(back_buf, zi, small),
-            b_s.at[zi], b_r.at[zi], (other, part),
+            own_sum.at[0], wide_buf.at[sender], w_s.at[sender], w_r.at[sender], (sender, part)
         )
 
-    def line_back(zi, small, half=0):
-        at = pl.ds(0, width) if small else columns(half)
+    def narrow(source, sender):
         return remote(
-            z_send.at[zi, :, at], z_buf.at[z, :, at],
-            z_s.at[half, zi], z_r.at[half, z], (2 * zi + x, part),
-        )
-
-    def line_got(zi, small, half=0):
-        at = pl.ds(0, width) if small else columns(half)
-        return remote(
-            z_send.at[zi, :, at], z_buf.at[zi, :, at],
-            z_s.at[half, zi], z_r.at[half, zi], (2 * zi + x, part),
+            narrow_send.at[source], narrow_buf.at[sender],
+            z_s.at[source], z_r.at[sender], (source, part),
         )
 
     def either(zi, act):
@@ -694,59 +686,45 @@
             added = (mine[source].astype(f32) + near_buf[source].astype(f32)).astype(bf16)
             if own:
                 own_sum[zi] = added
+
+                @pl.when((zi < z) | (zi > z))
+                def _():
+                    wide(source, True).start()
             else:
                 back_send[zi] = added
-                cross_back(zi, False).start()
+                wide(source, False).start()
 
         either(zi, act)
 
-    def half_sum(source, zi, own):
+    def half_sum(source, zi):
         @pl.when(is_far(zi))
         def _():
             half_over(source).wait_recv()
             at = columns(plane)
             added = mine[source, :, at].astype(f32) + near_buf[source, :, at].astype(f32)
-            added = (added + half_buf[source].astype(f32)).astype(bf16)
-            if own:
-                own_sum[zi, :, pl.ds(0, width)] = added
-            else:
-                back_send[zi, :, pl.ds(0, width)] = added
-                cross_back(zi, True).start()
-
-    def merge(i):
-        zi = place(i)
-        source = 2 * zi + x
-        tn = (((0,), (0,)), ((), ()))
-
-        def act(small):
-            cross_back(zi, small).wait_recv()
-            for half in range(1 if small else 2):
+            narrow_send[source] = (added + half_buf[source].astype(f32)).astype(bf16)
+            narrow(source, here).start()
+
+    tn = (((0,), (0,)), ((), ()))
+
+    def add_wide(sender, carry):
+        @pl.when(jnp.logical_not(is_far(sender // 2)) & ((sender < here) | (sender > here)))
+        def _():
+            wide_got(sender).wait_recv()
+            for half in range(2):
                 at = pl.ds(half * width, width)
-                added = lax.dot_general(
-                    pick(source, here), own_sum[zi, :, at], tn, preferred_element_type=f32
-                ) + lax.dot_general(
-                    pick(source, other), back_buf[zi, :, at], tn, preferred_element_type=f32
+                total[:, at] = total[:, at] + lax.dot_general(
+                    pick(here, sender), wide_buf[sender, :, at], tn, preferred_element_type=f32
                 )
-                if small:
-                    z_send[zi, :, at] = added.astype(bf16)
-                else:
-                    @pl.when(i == 0)
-                    def _():
-                        total[:, at] = added
-
-                    @pl.when(i >= 1)
-                    def _():
-                        z_send[zi, :, at] = added.astype(bf16)
-
-            if small:
-                line_back(zi, True).start()
-            else:
-                @pl.when(i >= 1)
-                def _():
-                    line_back(zi, False, 1 - plane).start()
-                    line_back(zi, False, plane).start()
-
-        either(zi, act)
+
+        return carry
+
+    def add_own():
+        for half in range(2):
+            at = pl.ds(half * width, width)
+            total[:, at] = lax.dot_general(
+                pick(here, here), own_sum[z, :, at], tn, preferred_element_type=f32
+            )
 
     def own_at(i):
         return 2 * place(i) + x
@@ -765,6 +743,10 @@
         def _():
             arrive(0, i - 1)
 
+        @pl.when(i == count)
+        def _():
+            pair_sum(own_at(last - 1), place(last - 1), True)
+
         @pl.when(i >= 2)
         def _():
             hand_on(other_at(i - 2))
@@ -784,7 +766,6 @@
 
         @pl.when(i == count)
         def _():
-            pair_sum(own_at(last - 1), place(last - 1), True)
             pair_sum(other_at(last - 1), place(last - 1), False)
 
         @pl.when(i < count)
@@ -813,6 +794,12 @@
         @pl.when((i == 2) & (middle == 1))
         def _():
             send_extra(1 - inward)
+            hand_on_extra(1)
+
+        @pl.when((i == 3) & (middle == 1))
+        def _():
+            compute(own_at(1), 0)
+            pair_sum(own_at(1), place(1), True)
 
         @pl.when(i >= 3)
         def _():
@@ -824,7 +811,7 @@
             def _():
                 hand_on(own_at(i - 1))
 
-        @pl.when(i == count)
+        @pl.when((i == count) & (middle == 0))
         def _():
             hand_on_extra(1)
 
@@ -848,13 +835,27 @@
         return carry
 
     def closing(j, carry):
-        is_other = middle + j - 2 * middle * j
-
-        @pl.when(is_other == 1)
-        def _():
+        @pl.when(j == 1)
+        def _():
+            half_sum(own_at(last - 1), place(last - 1))
             hand_on(other_at(last))
 
-        compute(own_at(1) + (other_at(last) - own_at(1)) * is_other, 0)
+        @pl.when((j == 1) | (middle == 0))
+        def _():
+            compute(own_at(1) + (other_at(last) - own_at(1)) * j, 0)
+
+        @pl.when((j == 0) & (middle == 0))
+        def _():
+            pair_sum(own_at(1), place(1), True)
+
+        @pl.when(j == 1)
+        def _():
+            small_near.start()
+            small_near.wait_recv()
+            found_sum[...] = found_loc[...] + found_near[...]
+            small_far.start()
+            pair_sum(other_at(last), place(last), False)
+
         return carry
 
     def weights(n, carry):
@@ -879,20 +880,12 @@
     chunks = model_width // 256
     lax.fori_loop(0, count + 1, body, 0)
     lax.fori_loop(0, 2, closing, 0)
-    small_near.start()
-    pair_sum(other_at(last), place(last), False)
-    pair_sum(own_at(1), place(1), True)
-    merge(1)
-    half_sum(other_at(last - 1), place(last - 1), False)
-    half_sum(own_at(last - 1), place(last - 1), True)
-    merge(0)
-    small_near.wait_recv()
-    found_sum[...] = found_loc[...] + found_near[...]
-    small_far.start()
-    lax.fori_loop(0, chunks // 4, weights, 0)
-    half_sum(own_at(last), place(last), True)
-    merge(last - 1)
-    half_sum(other_at(last), place(last), False)
+
+    @pl.when(middle == 1)
+    def _():
+        half_sum(own_at(last), place(last))
+
+    half_sum(other_at(last - 1), place(last - 1))
     small_far.wait_recv()
     found_send[...] = found_sum[...] + found_far[...]
     found_out[here] = found_send[here]
@@ -902,30 +895,28 @@
         return carry
 
     lax.fori_loop(1, ep_count, share, 0)
-    lax.fori_loop(chunks // 4, chunks, weights, 0)
-    merge(last)
-
-    def add(half):
-        def one(i, carry):
-            zi = order(i)
-
-            @pl.when(jnp.logical_not(is_far(zi)))
-            def _():
-                at = columns(half)
-                line_got(zi, False, half).wait_recv()
-                total[:, at] = total[:, at] + z_buf[zi, :, at].astype(f32)
-
-            return carry
-
-        lax.fori_loop(1, count, one, 0)
-
-    def add_far(i, carry):
-        zi = order(i)
-
-        @pl.when(is_far(zi))
-        def _():
-            line_got(zi, True).wait_recv()
-            total_half[...] = total_half[...] + z_buf[zi, :, pl.ds(0, width)].astype(f32)
+    add_own()
+    lax.fori_loop(0, chunks // 8, weights, 0)
+
+    @pl.when(middle == 0)
+    def _():
+        half_sum(own_at(last), place(last))
+
+    lax.fori_loop(chunks // 8, chunks // 4, weights, 0)
+    half_sum(other_at(last), place(last))
+    lax.fori_loop(chunks // 4, chunks // 4 + 1, weights, 0)
+    lax.fori_loop(0, ep_count, add_wide, 0)
+    y_send[...] = total[:, columns(1 - plane)].astype(bf16)
+    last_y.start()
+    lax.fori_loop(chunks // 4 + 1, chunks // 2, weights, 0)
+
+    def add_far(sender, carry):
+        @pl.when(is_far(sender // 2))
+        def _():
+            narrow(here, sender).wait_recv()
+            total_half[...] = total_half[...] + lax.dot_general(
+                pick(here, sender), narrow_buf[sender], tn, preferred_element_type=f32
+            )
 
         return carry
 
@@ -940,7 +931,6 @@
                 chain(kind, zi, 1).wait_send()
 
         cross_meta(zi).wait_send()
-        either(zi, lambda small: cross_back(zi, small).wait_send())
         for kind in range(2):
             cross(kind, zi).wait_send()
 
@@ -952,6 +942,10 @@
         @pl.when(is_far(source // 2))
         def _():
             half_over(source).wait_send()
+
+        @pl.when(jnp.logical_not(is_far(source // 2)) & ((source < here) | (source > here)))
+        def _():
+            wide(source, False).wait_send()
 
         @pl.when((source < here) | (source > here))
         def _():
@@ -973,12 +967,9 @@
         chain_extra(0, way).wait_send()
         chain_extra(1, way).wait_send()
 
-    add(1 - plane)
-    y_send[...] = total[:, columns(1 - plane)].astype(bf16)
-    last_y.start()
+    lax.fori_loop(chunks // 2, chunks, weights, 0)
     lax.fori_loop(0, count, finish, 0)
     lax.fori_loop(0, ep_count, finish_source, 0)
-    add(plane)
     finish_extra(inward)
 
     @pl.when(middle == 1)
@@ -992,28 +983,21 @@
         last_found(j).wait()
         return carry
 
-    lax.fori_loop(1, ep_count, finish_found, 0)
-    lax.fori_loop(1, count, add_far, 0)
+    lax.fori_loop(0, ep_count, add_far, 0)
     last_y.wait_recv()
     token_out[...] = (
         total[:, columns(plane)] + total_half[...] + y_buf[...].astype(f32)
     ).astype(bf16)
 
-    def finish_line(i, carry):
-        zi = order(i)
-
-        @pl.when(is_far(zi))
-        def _():
-            line_back(zi, True).wait_send()
-
-        @pl.when(jnp.logical_not(is_far(zi)))
-        def _():
-            line_back(zi, False, 0).wait_send()
-            line_back(zi, False, 1).wait_send()
-
-        return carry
-
-    lax.fori_loop(1, count, finish_line, 0)
+    def finish_narrow(source, carry):
+        @pl.when(is_far(source // 2))
+        def _():
+            narrow(source, here).wait_send()
+
+        return carry
+
+    lax.fori_loop(1, ep_count, finish_found, 0)
+    lax.fori_loop(0, ep_count, finish_narrow, 0)
     last_y.wait_send()
 
 
@@ -1048,11 +1032,11 @@
         vm((ep_count,) + half, bf16),
         vm((count,) + half, bf16),
         vm((count,) + half, bf16),
-        vm((count,) + half, bf16),
+        vm((ep_count,) + half, bf16),
         vm((ep_count, capacity, width), bf16),
         vm((ep_count, capacity, width), bf16),
-        vm((count, token_count, 2 * width), bf16),
-        vm((count, token_count, 2 * width), bf16),
+        vm((ep_count, capacity, width), bf16),
+        vm((ep_count, capacity, width), bf16),
         vm((token_count, 2 * width), f32),
         vm((token_count, width), f32),
         vm((token_count, width), bf16),
@@ -1067,8 +1051,8 @@
         dma((2, ep_count)), dma((2, ep_count)),
         dma((ep_count,)), dma((ep_count,)),
         dma((ep_count,)), dma((ep_count,)),
-        dma((count,)), dma((count,)),
-        dma((2, count)), dma((2, count)),
+        dma((ep_count,)), dma((ep_count,)),
+        dma((ep_count,)), dma((ep_count,)),
         dma((1,)), dma((1,)), dma((2,)), dma((2,)),
         dma((ep_count,)), dma((ep_count,)), dma((9,)),
     ]

time: 99.3 us -> 90.9 us (0.915)
  Pallas kernels: 98.4 us -> 89.9 us
    pallas_call x1, Pallas kernels: 95.7 us -> 87.2 us  [fused(): pl.pallas_call(fused_kernel, out_shape=(jax.ShapeDtypeStruct((token_count...]
where the time goes in v4:
time: 90.9 us; the launch traced here: 90.7 us
  Pallas kernels  89.9 us (99%)
    pallas_call x1, Pallas kernels, fused(): pl.pallas_call(fused_kernel, out_shape=(jax.ShapeDtypeStruct((token_count...  87.2 us
    pallas_call x1, Pallas kernels, store(): pl.pallas_call(store_kernel, out_shape=tuple(outs), in_specs=[pl.BlockSpe...  2.76 us

profile of v4, /device:TPU:0, one launch (start us, length us, event | category | flops | bytes accessed | tf_op | source)
XLA Modules:
  0.0 90.7 jit_solution(1231837480178225744)
XLA Ops:
  0.6 0.0 copy-start
  0.6 87.2 %shard_map.110 = (bf16[256,512]{1,0:T(8,128)(2,1)S(1)}, f32[8,1,256]{2,1,0:T(1,128)S(1)}, f32[2048,256]{1,0:T(8,128)S(1)}, f32[2048,256]{1,0:T(8,128)S(1)}, f32[256,2048]{1,0:T(8,128)S(1)}) custom-call(bf16[256,2048]{1,0:T(8,128)(2,1)} %tok_hbm.1, bf16[256,2048]{1,0:T(8,128)(2,1)} %grd_hbm.1, s32[4,256]{1,0:T(4,128)} %bitcast.9, f32[4,256]{1,0:T(4,128)} %bitcast.14, ...), custom_call_target="tpu_custom_call" | custom-call | tf_op jit(solution)/shard_map/pallas_call | solution.py:1059
  87.8 0.0 copy-done
  87.8 2.8 %shard_map.111 = (bf16[256,512]{1,0:T(8,128)(2,1)}, f32[4,256]{1,0:T(4,128)}, f32[2048,256]{1,0:T(8,128)}, f32[2048,256]{1,0:T(8,128)}, f32[256,2048]{1,0:T(8,128)}) custom-call(bf16[256,512]{1,0:T(8,128)(2,1)S(1)} %get-tuple-element.15.token_ref, f32[8,1,256]{2,1,0:T(1,128)S(1)} %get-tuple-element.16.found_ref, f32[2048,256]{1,0:T(8,128)S(1)} %get-tuple-element.17.gate_ref, ...), custom_call_target="tpu_custom_call" | custom-call | tf_op jit(solution)/shard_map/pallas_call | solution.py:1106
Async XLA Ops:
  0.6 87.2 %copy-start = (s32[256,4]{0,1:T(4,128)S(1)}, s32[256,4]{0,1:T(4,128)}, u32[]{:S(2)}) copy-start(s32[256,4]{0,1:T(4,128)} %param.8) | copy-start | bytes 12292

commit v5 on v4

--- a/solution.py
+++ b/solution.py
@@ -817,12 +817,13 @@
 
         @pl.when((i == 0) | (i >= 3))
         def _():
-            step = i - (i + count - 1) // count
+            step = i - (i + count - 1) // count - (1 - middle) * (i // count) * (last - 1)
             compute(own_at(step), 1 - (step + count - 1) // count)
 
         @pl.when(i == count)
         def _():
-            pair_sum(own_at(last), place(last), True)
+            step = 1 + middle * (last - 1)
+            pair_sum(own_at(step), place(step), True)
 
         @pl.when(i == 1)
         def _():
@@ -842,11 +843,11 @@
 
         @pl.when((j == 1) | (middle == 0))
         def _():
-            compute(own_at(1) + (other_at(last) - own_at(1)) * j, 0)
+            compute(own_at(last) + (other_at(last) - own_at(last)) * j, 0)
 
         @pl.when((j == 0) & (middle == 0))
         def _():
-            pair_sum(own_at(1), place(1), True)
+            pair_sum(own_at(last), place(last), True)
 
         @pl.when(j == 1)
         def _():
@@ -983,6 +984,7 @@
         last_found(j).wait()
         return carry
 
+    lax.fori_loop(1, ep_count, finish_found, 0)
     lax.fori_loop(0, ep_count, add_far, 0)
     last_y.wait_recv()
     token_out[...] = (
@@ -996,7 +998,6 @@
 
         return carry
 
-    lax.fori_loop(1, ep_count, finish_found, 0)
     lax.fori_loop(0, ep_count, finish_narrow, 0)
     last_y.wait_send()
 

time: 90.9 us -> 90.7 us (level)
  no operation moved by 1% of the time
where the time goes in v5:
time: 90.7 us; the launch traced here: 90.6 us
  Pallas kernels  89.7 us (99%)
    pallas_call x1, Pallas kernels, fused(): pl.pallas_call(fused_kernel, out_shape=(jax.ShapeDtypeStruct((token_count...  87 us
    pallas_call x1, Pallas kernels, store(): pl.pallas_call(store_kernel, out_shape=tuple(outs), in_specs=[pl.BlockSpe...  2.76 us

profile of v5, /device:TPU:0, one launch (start us, length us, event | category | flops | bytes accessed | tf_op | source)
XLA Modules:
  0.0 90.6 jit_solution(18182477571427752735)
XLA Ops:
  0.6 0.0 copy-start
  0.6 87.0 %shard_map.110 = (bf16[256,512]{1,0:T(8,128)(2,1)S(1)}, f32[8,1,256]{2,1,0:T(1,128)S(1)}, f32[2048,256]{1,0:T(8,128)S(1)}, f32[2048,256]{1,0:T(8,128)S(1)}, f32[256,2048]{1,0:T(8,128)S(1)}) custom-call(bf16[256,2048]{1,0:T(8,128)(2,1)} %tok_hbm.1, bf16[256,2048]{1,0:T(8,128)(2,1)} %grd_hbm.1, s32[4,256]{1,0:T(4,128)} %bitcast.9, f32[4,256]{1,0:T(4,128)} %bitcast.14, ...), custom_call_target="tpu_custom_call" | custom-call | tf_op jit(solution)/shard_map/pallas_call | solution.py:1060
  87.6 0.0 copy-done
  87.6 2.8 %shard_map.111 = (bf16[256,512]{1,0:T(8,128)(2,1)}, f32[4,256]{1,0:T(4,128)}, f32[2048,256]{1,0:T(8,128)}, f32[2048,256]{1,0:T(8,128)}, f32[256,2048]{1,0:T(8,128)}) custom-call(bf16[256,512]{1,0:T(8,128)(2,1)S(1)} %get-tuple-element.15.token_ref, f32[8,1,256]{2,1,0:T(1,128)S(1)} %get-tuple-element.16.found_ref, f32[2048,256]{1,0:T(8,128)S(1)} %get-tuple-element.17.gate_ref, ...), custom_call_target="tpu_custom_call" | custom-call | tf_op jit(solution)/shard_map/pallas_call | solution.py:1107
Async XLA Ops:
  0.6 87.0 %copy-start = (s32[256,4]{0,1:T(4,128)S(1)}, s32[256,4]{0,1:T(4,128)}, u32[]{:S(2)}) copy-start(s32[256,4]{0,1:T(4,128)} %param.8) | copy-start | bytes 12292

commit v6 on v5

--- a/solution.py
+++ b/solution.py
@@ -985,20 +985,20 @@
         return carry
 
     lax.fori_loop(1, ep_count, finish_found, 0)
+    def finish_narrow(source, carry):
+        @pl.when(is_far(source // 2))
+        def _():
+            narrow(source, here).wait_send()
+
+        return carry
+
+    lax.fori_loop(0, ep_count, finish_narrow, 0)
     lax.fori_loop(0, ep_count, add_far, 0)
     last_y.wait_recv()
     token_out[...] = (
         total[:, columns(plane)] + total_half[...] + y_buf[...].astype(f32)
     ).astype(bf16)
 
-    def finish_narrow(source, carry):
-        @pl.when(is_far(source // 2))
-        def _():
-            narrow(source, here).wait_send()
-
-        return carry
-
-    lax.fori_loop(0, ep_count, finish_narrow, 0)
     last_y.wait_send()
 
 

time: 90.7 us -> 90.6 us (level)
  no operation moved by 1% of the time
where the time goes in v6:
time: 90.6 us; the launch traced here: 90.5 us
  Pallas kernels  89.6 us (99%)
    pallas_call x1, Pallas kernels, fused(): pl.pallas_call(fused_kernel, out_shape=(jax.ShapeDtypeStruct((token_count...  86.9 us
    pallas_call x1, Pallas kernels, store(): pl.pallas_call(store_kernel, out_shape=tuple(outs), in_specs=[pl.BlockSpe...  2.76 us

profile of v6, /device:TPU:0, one launch (start us, length us, event | category | flops | bytes accessed | tf_op | source)
XLA Modules:
  0.0 90.5 jit_solution(4023980806822721336)
XLA Ops:
  0.6 0.0 copy-start
  0.6 86.9 %shard_map.110 = (bf16[256,512]{1,0:T(8,128)(2,1)S(1)}, f32[8,1,256]{2,1,0:T(1,128)S(1)}, f32[2048,256]{1,0:T(8,128)S(1)}, f32[2048,256]{1,0:T(8,128)S(1)}, f32[256,2048]{1,0:T(8,128)S(1)}) custom-call(bf16[256,2048]{1,0:T(8,128)(2,1)} %tok_hbm.1, bf16[256,2048]{1,0:T(8,128)(2,1)} %grd_hbm.1, s32[4,256]{1,0:T(4,128)} %bitcast.9, f32[4,256]{1,0:T(4,128)} %bitcast.14, ...), custom_call_target="tpu_custom_call" | custom-call | tf_op jit(solution)/shard_map/pallas_call | solution.py:1060
  87.5 0.0 copy-done
  87.5 2.8 %shard_map.111 = (bf16[256,512]{1,0:T(8,128)(2,1)}, f32[4,256]{1,0:T(4,128)}, f32[2048,256]{1,0:T(8,128)}, f32[2048,256]{1,0:T(8,128)}, f32[256,2048]{1,0:T(8,128)}) custom-call(bf16[256,512]{1,0:T(8,128)(2,1)S(1)} %get-tuple-element.15.token_ref, f32[8,1,256]{2,1,0:T(1,128)S(1)} %get-tuple-element.16.found_ref, f32[2048,256]{1,0:T(8,128)S(1)} %get-tuple-element.17.gate_ref, ...), custom_call_target="tpu_custom_call" | custom-call | tf_op jit(solution)/shard_map/pallas_call | solution.py:1107
Async XLA Ops:
  0.6 86.9 %copy-start = (s32[256,4]{0,1:T(4,128)S(1)}, s32[256,4]{0,1:T(4,128)}, u32[]{:S(2)}) copy-start(s32[256,4]{0,1:T(4,128)} %param.8) | copy-start | bytes 12292
